TPU v7x, 256 devices: a whole 4x4x8 slice. The times are simulated.
256 devices in a mesh: sp: 32 (over z, y), tp: 8 (over x, core).
Axes of the slice: x: 4, y: 4, z: 8, core: 2. Of those that a mesh axis runs over, the one named last changes fastest.
Arguments:
- residual: bfloat16 [32768, 2048], P(('sp', 'tp')), may hold values from -6 to 6
- first_group_queries: bfloat16 [32768, 1024], P('sp', 'tp'), may hold values from -6 to 6
- first_group_keys: bfloat16 [32768, 1024], P('sp', 'tp'), may hold values from -6 to 6
- second_group_queries: bfloat16 [32768, 512], P('sp', 'tp'), may hold values from -6 to 6
- second_group_keys: bfloat16 [32768, 512], P('sp', 'tp'), may hold values from -6 to 6
- primary_retain_switch_inputs: bfloat16 [32768, 1024], P('sp', 'tp'), may hold values from -12 to 16
- secondary_retain_switch_inputs: bfloat16 [32768, 512], P('sp', 'tp'), may hold values from -12 to 16
- timestep_fading_exponent: float32 [32768], P('sp'), may hold values from -2.1 to 0
- values: bfloat16 [2, 32768, 1024], P(None, 'sp', 'tp'), may hold values from -6 to 6
- output_gate_logits: bfloat16 [2, 32768, 1024], P(None, 'sp', 'tp'), may hold values from -6 to 6
- head_norm_gains: float32 [2, 1024], P(None, 'tp'), may hold values from 0.1 to 1.9
- output_projection: bfloat16 [2, 1024, 2048], P(None, 'tp'), may hold values from -0.125 to 0.125
- feedforward_norm_gain: float32 [2048], replicated, may hold values from 0.1 to 1.9
- gate_projection: bfloat16 [2048, 6144], P('sp', 'tp'), may hold values from -0.125 to 0.125
- up_projection: bfloat16 [2048, 6144], P('sp', 'tp'), may hold values from -0.125 to 0.125
- down_projection: bfloat16 [6144, 2048], P('tp', 'sp'), may hold values from -0.078125 to 0.078125
Outputs:
- layer_out: bfloat16 [32768, 2048], P(('sp', 'tp'))
All inputs are finite; a program needn't handle non-finite values.
Results may differ from a plain program's by a relative error of at most 0.018.
Values may be sent and summed in bfloat16 or wider, within the bound.
A program may use at most 128 MiB of HBM per device.

v0:
```python
import jax
import jax.numpy as jnp
from jax import lax
from jax.sharding import Mesh
from jax.sharding import PartitionSpec as P

FIRST_KEY_SIZE = 128
SECOND_KEY_SIZE = 64
DV = 128
BLOCK = 64
SP = ("sp_0", "sp_1")
TP = ("tp_0", "tp_1")
SP_TP = ("sp_0", "sp_1", "tp_0", "tp_1")


EPS = 1e-06
SOFTNESS_SCALE = 16.0


def in_one_piece(arrays, axis, dim, along):
    ends, at = ([], 0)
    for a in arrays[:-1]:
        at += a.shape[along]
        ends.append(at)
    both = jnp.concatenate(arrays, axis=along)
    return tuple(jnp.split(lax.all_gather(both, axis, axis=dim, tiled=True), ends, axis=along))


def gather_axes(shard, axes, dim):
    result = shard
    for number in range(len(axes) - 1, -1, -1):
        result = lax.all_gather(result, axes[number], axis=dim, tiled=True)
    return result


def filled_with(shard, identity):
    return jax.tree.map(
        lambda a, e: jnp.broadcast_to(jnp.asarray(e, a.dtype), a.shape), shard, identity
    )


def gathered_once(shard, axis):
    leaves = jax.tree.leaves(shard)
    sequence = sorted(range(len(leaves)), key=lambda k: -leaves[k].size)
    width = (1, *leaves[sequence[0]].shape)[-1]
    lines = [
        jnp.pad(leaves[k].reshape(-1), (0, -leaves[k].size % width)).reshape(-1, width)
        for k in sequence
    ]
    both, at, found = (lax.all_gather(jnp.concatenate(lines), axis), 0, {})
    for k, line in zip(sequence, lines):
        piece = both[:, at : at + len(line)].reshape(len(both), -1)
        found[k] = piece[:, : leaves[k].size].reshape(-1, *leaves[k].shape)
        at += len(line)
    numbers = iter(range(len(leaves)))
    return jax.tree.map(lambda _: found[next(numbers)], shard)


def prefix_by_axis(shard, axes, combine, identity):
    before = start = filled_with(shard, identity)
    so_far = shard
    for axis in reversed(axes):
        peers, place = (lax.axis_size(axis), lax.axis_index(axis))
        pieces = gathered_once(
            jax.tree.map(
                lambda part, kind: part.astype(kind),
                so_far,
                (jnp.bfloat16, jnp.bfloat16, jnp.bfloat16, jnp.bfloat16),
            ),
            axis,
        )
        inside, so_far = (start, start)
        for k in range(peers):
            passed = k < place
            so_far = combine(
                so_far, jax.tree.map(lambda part, own: part[k].astype(own.dtype), pieces, shard)
            )
            inside = jax.tree.map(lambda new, old: jnp.where(passed, new, old), so_far, inside)
        before = combine(inside, before)
    return before


def in_blocks(shard, dim, peers):
    dims = shard.shape
    pieces = shard.reshape(*dims[:dim], peers, dims[dim] // peers, *dims[dim + 1 :])
    return jnp.moveaxis(pieces, dim, 0)


def summed_on_arrival(shard, axis, dim):
    peers = lax.axis_size(axis)
    pieces = lax.all_to_all(in_blocks(shard, dim, peers), axis, 0, 0, tiled=True)
    return jnp.sum(pieces.astype(jnp.float32), axis=0)


def summed_rows(shard, axes, dim):
    far, near = axes
    own = summed_on_arrival(in_blocks(shard, dim, lax.axis_size(far)), near, dim + 1)
    return jnp.sum(
        lax.all_to_all(own.astype(jnp.bfloat16), far, 0, 0, tiled=True).astype(jnp.float32), axis=0
    )


def sent_to_all(shard, axis):
    copies = jnp.broadcast_to(shard, (lax.axis_size(axis), *shard.shape))
    return lax.all_to_all(copies, axis, split_axis=0, concat_axis=0, tiled=True)


def laid_out(pieces, dim):
    pieces = jnp.moveaxis(pieces, 0, dim)
    dims = pieces.shape
    return pieces.reshape(*dims[:dim], dims[dim] * dims[dim + 1], *dims[dim + 2 :])


def whole_of(shard, axes, dim):
    far, near = axes
    pieces = sent_to_all(sent_to_all(shard, far), near)
    return laid_out(pieces.swapaxes(0, 1).reshape(-1, *shard.shape), dim)


def blocks(source, block_count, head_count, key_width):
    return (
        source.astype(jnp.float32)
        .reshape(block_count, BLOCK, head_count, key_width)
        .transpose(0, 2, 1, 3)
    )


def within_block_pass(
    query_matrix_rows,
    key_matrix_rows,
    value_matrix_rows,
    retain_switch_lines,
    position_decay_rows,
    key_width,
):
    head_count = query_matrix_rows.shape[1] // key_width
    block_count = query_matrix_rows.shape[0] // BLOCK
    decay_logarithm = (
        jax.nn.log_sigmoid(retain_switch_lines.astype(jnp.float32)) / SOFTNESS_SCALE
        + position_decay_rows[:, None]
    )
    query_blocks = blocks(query_matrix_rows, block_count, head_count, key_width) * key_width ** (
        -0.5
    )
    key_blocks = blocks(key_matrix_rows, block_count, head_count, key_width)
    value_blocks = blocks(value_matrix_rows, block_count, head_count, DV)
    decay_blocks = jnp.cumsum(blocks(decay_logarithm, block_count, head_count, key_width), axis=2)
    causal = jnp.tril(jnp.ones((BLOCK, BLOCK), dtype=bool))

    def advance(running_state, inputs):
        query_piece, key_piece, value_piece, decay_piece = inputs
        spread_log = decay_piece[:, :, None, :] - decay_piece[:, None, :, :]
        decay_grid = jnp.exp(jnp.where(causal[None, :, :, None], spread_log, -jnp.inf))
        scores = jnp.sum(
            query_piece[:, :, None, :] * key_piece[:, None, :, :] * decay_grid, axis=-1
        )
        block_result = jnp.einsum("hij,hjv->hiv", scores, value_piece)
        block_result = block_result + jnp.einsum(
            "rus,rsp->rup", query_piece * jnp.exp(decay_piece), running_state
        )
        final_log_decay = decay_piece[:, -1:, :]
        running_state = jnp.exp(final_log_decay[:, 0, :])[:, :, None] * running_state + jnp.einsum(
            "qxe,qxt->qet", key_piece * jnp.exp(final_log_decay - decay_piece), value_piece
        )
        return (running_state, block_result)

    zero_state = jnp.zeros((head_count, key_width, DV), jnp.float32)
    local_state, local_out = lax.scan(
        advance, zero_state, (query_blocks, key_blocks, value_blocks, decay_blocks)
    )
    block_totals = decay_blocks[:, :, -1, :]
    before_log = jnp.cumsum(block_totals, axis=0) - block_totals
    cross_block_term = query_blocks * jnp.exp(decay_blocks + before_log[:, :, None, :])
    decay_total = jnp.exp(jnp.sum(block_totals, axis=0))
    return (local_out, cross_block_term, decay_total, local_state)


def finish(local_out, cross_block_term, incoming_state, gate_rows, gain_row):
    carried_over = jnp.einsum("pjli,jie->pjle", cross_block_term, incoming_state)
    summed = (local_out + carried_over).transpose(0, 2, 1, 3)
    row_count = summed.shape[0] * summed.shape[1]
    summed = summed.reshape(row_count, summed.shape[2], summed.shape[3])
    inverse = lax.rsqrt(jnp.mean(summed * summed, axis=-1, keepdims=True) + EPS)
    normed = (summed * inverse).reshape(row_count, -1) * gain_row
    return (jax.nn.silu(gate_rows.astype(jnp.float32)) * normed).astype(jnp.bfloat16)


def join_states(earlier, after_part):
    return (
        earlier[0] * after_part[0],
        after_part[0][:, :, None] * earlier[1] + after_part[1],
        earlier[2] * after_part[2],
        after_part[2][:, :, None] * earlier[3] + after_part[3],
    )


def row_norm(source, gain_row):
    widened = source.astype(jnp.float32)
    inverse = lax.rsqrt(jnp.mean(widened * widened, axis=-1, keepdims=True) + EPS)
    return (widened * inverse * gain_row).astype(jnp.bfloat16)


def per_device(
    residual,
    first_group_queries,
    first_group_keys,
    second_group_queries,
    second_group_keys,
    primary_retain_switch_inputs,
    secondary_retain_switch_inputs,
    timestep_fading_exponent,
    values,
    output_gate_logits,
    head_norm_gains,
    output_projection,
    feedforward_norm_gain,
    gate_projection,
    up_projection,
    down_projection,
):
    inner_weights = in_one_piece((gate_projection, up_projection), SP, 0, 1)
    outer_weight = gather_axes(down_projection, SP, 1)
    out_a, reach_a, decay_a, state_a = within_block_pass(
        first_group_queries,
        first_group_keys,
        values[0],
        primary_retain_switch_inputs,
        timestep_fading_exponent,
        FIRST_KEY_SIZE,
    )
    out_b, reach_b, decay_b, state_b = within_block_pass(
        second_group_queries,
        second_group_keys,
        values[1],
        secondary_retain_switch_inputs,
        timestep_fading_exponent,
        SECOND_KEY_SIZE,
    )
    identity = (
        jnp.ones_like(decay_a),
        jnp.zeros_like(state_a),
        jnp.ones_like(decay_b),
        jnp.zeros_like(state_b),
    )
    incoming_state = prefix_by_axis((decay_a, state_a, decay_b, state_b), SP, join_states, identity)
    gated_a = finish(out_a, reach_a, incoming_state[1], output_gate_logits[0], head_norm_gains[0])
    gated_b = finish(out_b, reach_b, incoming_state[3], output_gate_logits[1], head_norm_gains[1])
    attention = summed_rows(
        (
            jnp.dot(gated_a, output_projection[0], preferred_element_type=jnp.float32)
            + jnp.dot(gated_b, output_projection[1], preferred_element_type=jnp.float32)
        ).astype(jnp.bfloat16),
        ("tp_0", "tp_1"),
        0,
    )
    mid_rows = (residual.astype(jnp.float32) + attention).astype(jnp.bfloat16)
    all_rows = whole_of(row_norm(mid_rows, feedforward_norm_gain), ("tp_0", "tp_1"), 0)
    gate_sum = jnp.dot(all_rows, inner_weights[0], preferred_element_type=jnp.float32)
    up_sum = jnp.dot(all_rows, inner_weights[1], preferred_element_type=jnp.float32)
    hidden = (jax.nn.silu(gate_sum) * up_sum).astype(jnp.bfloat16)
    down_terms = jnp.dot(hidden, outer_weight, preferred_element_type=jnp.float32)
    down_sum = summed_rows(down_terms.astype(jnp.bfloat16), ("tp_0", "tp_1"), 0)
    return (mid_rows.astype(jnp.float32) + down_sum).astype(jnp.bfloat16)


def solution(mesh):
    finer = Mesh(mesh.devices.reshape(8, 4, 4, 2), ("sp_0", "sp_1", "tp_0", "tp_1"))
    return jax.shard_map(
        per_device,
        mesh=finer,
        in_specs=(
            P(SP_TP, None),
            P(SP, TP),
            P(SP, TP),
            P(SP, TP),
            P(SP, TP),
            P(SP, TP),
            P(SP, TP),
            P(SP),
            P(None, SP, TP),
            P(None, SP, TP),
            P(None, TP),
            P(None, TP, None),
            P(),
            P(SP, TP),
            P(SP, TP),
            P(TP, SP),
        ),
        out_specs=P(SP_TP, None),
        check_vma=False,
    )
```

profile of v0, /device:TPU:1, one launch (start us, length us, event | category | flops | bytes accessed | tf_op | source)
XLA Modules:
  0.0 337.3 jit_solution(4332718211010056057)
XLA Ops:
  6.5 1.7 pad_maximum_fusion
  8.3 13.1 %all_gather.26 = bf16[768,256]{0,1:T(8,128)(2,1)} all-gather(bf16[768,64]{0,1:T(8,128)(2,1)} %param.35), channel_id=1, replica_groups=mesh['sp_0'=8,'sp_1'=4,'tp_0'=4,'tp_1'=2] {'sp_1'}, dimensions={1}, use_global_device_ids=true | all-gather | bytes 491520 | tf_op jit(solution)/shard_map/all_gather | solution.py:32
  23.1 6.3 %fusion.274 = f32[16,1,64,64]{3,0,1,2:T(8,128)S(1)} fusion(f32[16,1,64,64]{3,0,1,2:T(8,128)S(1)} %copy.111), kind=kOutput, calls=%fused_computation.378 | output fusion | flops 4128768 | bytes 524288 | tf_op jit(solution)/shard_map/jit(cumsum)/reduce_window_sum | solution.py:147
  31.5 30.5 %while.27 = (s32[]{:T(128)}, f32[1,64,128]{2,1,0:T(8,128)S(1)}, f32[16,1,64,128]{3,2,1,0:T(8,128)S(1)}, f32[16,1,64,64]{3,0,1,2:T(8,128)S(1)}, f32[16,1,64,64]{3...) while((s32[]{:T(128)}, f32[1,64,128]{2,1,0:T(8,128)S(1)}, ...), condition=%wide.region_7.8_spmd.clone, body=%wide.region_5.7_spmd.clone.sunk | while | flops 4509699 | bytes 544884 | solution.py:168
  33.5 1.4 multiply_reduce_fusion.7
  35.4 1.4 multiply_reduce_fusion.7
  37.3 1.4 multiply_reduce_fusion.7
  39.2 1.4 multiply_reduce_fusion.7
  43.0 1.4 multiply_reduce_fusion.7
  44.9 1.4 multiply_reduce_fusion.7
  46.8 1.4 multiply_reduce_fusion.7
  48.7 1.4 multiply_reduce_fusion.7
  52.5 1.4 multiply_reduce_fusion.7
  54.4 1.4 multiply_reduce_fusion.7
  63.9 63.6 %while.26 = (s32[]{:T(128)}, f32[1,128,128]{2,1,0:T(8,128)S(1)}, f32[16,1,64,128]{3,2,1,0:T(8,128)}, f32[16,1,64,128]{3,0,1,2:T(8,128)S(1)}, f32[16,1,64,128]{3,...) while((s32[]{:T(128)}, f32[1,128,128]{2,1,0:T(8,128)S(1)}, ...), condition=%wide.region_3.4_spmd.clone, body=%wide.region_1.3_spmd.clone.sunk | while | flops 7962627 | bytes 783984 | solution.py:168
  127.6 10.6 %all-gather.2 = bf16[4,194,128]{2,1,0:T(8,128)(2,1)S(1)} all-gather(bf16[1,194,128]{2,1,0:T(8,128)(2,1)S(1)} %maximum_bitcast_fusion), channel_id=2, replica_groups=mesh['sp_0'=8,'sp_1'=4,'tp_0'=4,'tp_1'=2] {'sp_1'}, dimensions={0}, use_global_device_ids=true | all-gather | bytes 248320 | tf_op jit(solution)/shard_map/all_gather | solution.py:50
  138.5 21.8 %all-gather.3 = bf16[8,194,128]{2,1,0:T(8,128)(2,1)S(1)} all-gather(bf16[1,194,128]{2,1,0:T(8,128)(2,1)S(1)} %maximum_bitcast_fusion.1), channel_id=3, replica_groups=mesh['sp_0'=8,'sp_1'=4,'tp_0'=4,'tp_1'=2] {'sp_0'}, dimensions={0}, use_global_device_ids=true | all-gather | bytes 446976 | tf_op jit(solution)/shard_map/all_gather | solution.py:50
  162.6 2.2 multiply_reduce_fusion.3
  165.8 1.4 multiply_reduce_fusion.2
  167.3 1.6 fusion.94
  171.8 19.6 %all_to_all.30 = bf16[2,4,128,2048]{3,2,1,0:T(8,128)(2,1)} all-to-all(bf16[2,4,128,2048]{3,2,1,0:T(8,128)(2,1)S(1)} %bitcast.362), channel_id=1, replica_groups=mesh['sp_0'=8,'sp_1'=4,'tp_0'=4,'tp_1'=2] {'tp_1'}, dimensions={0} | all-to-all | bytes 8388608 | tf_op jit(solution)/shard_map/all_to_all | solution.py:91
  191.4 3.5 %reduce_sum.109 = bf16[4,128,2048]{2,1,0:T(8,128)(2,1)S(1)} reduce(bf16[2,4,128,2048]{3,2,1,0:T(8,128)(2,1)} %all_to_all.30, bf16[]{:T(256)} %constant.103.clone.1), dimensions={0}, to_apply=%region_14.15 | reduce | flops 1048576 | bytes 6291458 | tf_op jit(solution)/shard_map/reduce_sum | solution.py:92
  195.0 29.4 %all_to_all.31 = bf16[4,128,2048]{2,1,0:T(8,128)(2,1)S(1)} all-to-all(bf16[4,128,2048]{2,1,0:T(8,128)(2,1)S(1)} %reduce_sum.109), channel_id=1, replica_groups=mesh['sp_0'=8,'sp_1'=4,'tp_0'=4,'tp_1'=2] {'tp_0'}, dimensions={0} | all-to-all | bytes 4194304 | tf_op jit(solution)/shard_map/all_to_all | solution.py:99
  225.6 27.1 %all_to_all.32 = bf16[4,128,2048]{2,1,0:T(8,128)(2,1)S(1)} all-to-all(bf16[4,128,2048]{2,1,0:T(8,128)(2,1)S(1)} %broadcast_in_dim.56), channel_id=1, replica_groups=mesh['sp_0'=8,'sp_1'=4,'tp_0'=4,'tp_1'=2] {'tp_0'}, dimensions={0} | all-to-all | bytes 4194304 | tf_op jit(solution)/shard_map/all_to_all | solution.py:105
  253.2 9.4 %all_to_all.33 = bf16[2,4,128,2048]{3,2,1,0:T(8,128)(2,1)S(1)} all-to-all(bf16[2,4,128,2048]{3,2,1,0:T(8,128)(2,1)S(1)} %broadcast_in_dim.57), channel_id=1, replica_groups=mesh['sp_0'=8,'sp_1'=4,'tp_0'=4,'tp_1'=2] {'tp_1'}, dimensions={0} | all-to-all | bytes 8388608 | tf_op jit(solution)/shard_map/all_to_all | solution.py:105
  262.6 2.3 copy.127
  265.0 8.2 %fusion.58 = f32[1024,768]{1,0:T(8,128)} fusion(bf16[1024,2048]{1,0:T(8,128)(2,1)} %bitcast.374, bf16[2048,1536]{1,0:T(8,128)(2,1)} %all-gather.7.cloned.1.call-done), kind=kOutput, calls=%fused_computation.78 | convolution fusion | flops 3221225472 | bytes 10485760 | tf_op jit(solution)/shard_map/dot_general | solution.py:259
  273.1 13.2 %convolution_convert_fusion = bf16[1024,2048]{1,0:T(8,128)(2,1)} fusion(bf16[768,2048]{0,1:T(8,128)(2,1)} %all-gather.9.cloned.1.call-done, f32[1024,768]{1,0:T(8,128)} %fusion.58, bf16[1024,2048]{1,0:T(8,128)(2,1)} %bitcast.375, bf16[2048,1536]{1,0:T(8,128)(2,1)} %all-gather.7.cloned.1.call-done), kind=kOutput, calls=%fused_computation.77 | convolution fusion | flops 6449266688 | bytes 17825792 | tf_op jit(solution)/shard_map/dot_general | solution.py:261
  286.4 2.5 copy.141
  288.9 8.2 %all_to_all.34 = bf16[2,4,128,2048]{3,2,1,0:T(8,128)(2,1)} all-to-all(bf16[2,4,128,2048]{3,2,1,0:T(8,128)(2,1)S(1)} %bitcast.363), channel_id=1, replica_groups=mesh['sp_0'=8,'sp_1'=4,'tp_0'=4,'tp_1'=2] {'tp_1'}, dimensions={0} | all-to-all | bytes 8388608 | tf_op jit(solution)/shard_map/all_to_all | solution.py:91
  297.0 3.5 %reduce_sum.112 = bf16[4,128,2048]{2,1,0:T(8,128)(2,1)S(1)} reduce(bf16[2,4,128,2048]{3,2,1,0:T(8,128)(2,1)} %all_to_all.34, bf16[]{:T(256)} %constant.103.clone.1), dimensions={0}, to_apply=%region_17.18 | reduce | flops 1048576 | bytes 6291458 | tf_op jit(solution)/shard_map/reduce_sum | solution.py:92
  300.6 28.5 %all_to_all.35 = bf16[4,128,2048]{2,1,0:T(8,128)(2,1)S(1)} all-to-all(bf16[4,128,2048]{2,1,0:T(8,128)(2,1)S(1)} %reduce_sum.112), channel_id=1, replica_groups=mesh['sp_0'=8,'sp_1'=4,'tp_0'=4,'tp_1'=2] {'tp_0'}, dimensions={0} | all-to-all | bytes 4194304 | tf_op jit(solution)/shard_map/all_to_all | solution.py:99
  (377 shorter events, 94.0 us)
Async XLA Ops:
  6.5 23.0 %copy-start.9 = (f32[1024]{0:T(1024)S(1)}, f32[1024]{0:T(1024)}, u32[]{:S(2)}) copy-start(f32[1024]{0:T(1024)} %param.27) | copy-start | bytes 12292
  6.5 23.0 %copy-start.7 = (bf16[1024,128]{1,0:T(8,128)(2,1)S(1)}, bf16[1024,128]{1,0:T(8,128)(2,1)}, u32[]{:S(2)}) copy-start(bf16[1024,128]{1,0:T(8,128)(2,1)} %param.25) | copy-start | bytes 786436
  6.5 258.4 %all-gather.7.cloned.1.call-start = ((), (), s32[]{:S(2)}) async-start(), calls=%async_computation.6 | async-start | bytes 6488064 | tf_op jit(solution)/shard_map/all_gather | solution.py:26
  8.2 22.1 %copy-start.4 = (bf16[2,1024,128]{2,1,0:T(8,128)(2,1)S(1)}, bf16[2,1024,128]{2,1,0:T(8,128)(2,1)}, u32[]{:S(2)}) copy-start(bf16[2,1024,128]{2,1,0:T(8,128)(2,1)} %param.28) | copy-start | bytes 1572868
  8.2 264.9 %all-gather.9.cloned.1.call-start = ((), (), s32[]{:S(2)}) async-start(), calls=%async_computation.7 | async-start | bytes 3538944 | tf_op jit(solution)/shard_map/all_gather | solution.py:32
  21.5 9.6 %copy-start.5 = (bf16[1024,64]{0,1:T(8,128)(2,1)S(1)}, bf16[1024,64]{0,1:T(8,128)(2,1)}, u32[]{:S(2)}) copy-start(bf16[1024,64]{0,1:T(8,128)(2,1)} %param.23) | copy-start | bytes 393220
  22.7 8.5 %copy-start.8 = (bf16[1024,64]{0,1:T(8,128)(2,1)S(1)}, bf16[1024,64]{0,1:T(8,128)(2,1)}, u32[]{:S(2)}) copy-start(bf16[1024,64]{0,1:T(8,128)(2,1)} %param.24) | copy-start | bytes 393220
  31.4 30.6 %copy-start.1 = (bf16[1024,128]{1,0:T(8,128)(2,1)S(1)}, bf16[1024,128]{1,0:T(8,128)(2,1)}, u32[]{:S(2)}) copy-start(bf16[1024,128]{1,0:T(8,128)(2,1)} %param.21) | copy-start | bytes 786436
  127.5 35.1 %copy-start.3 = (f32[16,1,64,128]{3,2,1,0:T(8,128)S(1)}, f32[16,1,64,128]{3,2,1,0:T(8,128)}, u32[]{:S(2)}) copy-start(f32[16,1,64,128]{3,2,1,0:T(8,128)} %get-tuple-element.91) | copy-start | bytes 1572868
  160.3 0.8 copy-start.6
  162.6 4.7 %copy-start.11 = (f32[2,128]{1,0:T(2,128)S(1)}, f32[2,128]{1,0:T(2,128)}, u32[]{:S(2)}) copy-start(f32[2,128]{1,0:T(2,128)} %param.30) | copy-start | bytes 3076
  165.2 3.7 %copy-start = (bf16[2,128,2048]{2,1,0:T(8,128)(2,1)S(1)}, bf16[2,128,2048]{2,1,0:T(8,128)(2,1)}, u32[]{:S(2)}) copy-start(bf16[2,128,2048]{2,1,0:T(8,128)(2,1)} %param.31) | copy-start | bytes 3145732
  195.0 29.8 %copy-start.2 = (bf16[128,2048]{1,0:T(8,128)(2,1)S(1)}, bf16[128,2048]{1,0:T(8,128)(2,1)}, u32[]{:S(2)}) copy-start(bf16[128,2048]{1,0:T(8,128)(2,1)} %param.20) | copy-start | bytes 1572868
  224.4 0.7 copy-start.10
Sparse Core Ops, SparseCore 0:
  9.9 91.4 all-gather.6
  103.2 42.0 all-gather.8
where the time goes:
time: 341 us; the launch traced here: 337 us
  blocking collectives  168 us (49%)
  matrix products  75.1 us (22%)
  other arithmetic  65.8 us (19%)
  between operations  13.9 us (4%)
  local copies, waits for them, and re-layouts  13.2 us (4%)
    all_to_all x2, blocking collectives, summed_rows(): lax.all_to_all(own.astype(jnp.bfloat16), far, 0, 0, tiled=True)  58 us
    reduce_sum x32, other arithmetic, advance(): jnp.sum(query_piece[:, :, None, :] * key_piece[:, None, :, :] * decay_gri...  43.1 us
    all_to_all x2, blocking collectives, sent_to_all(): return lax.all_to_all(copies, axis, split_axis=0, concat_axis=0, tiled=True)  36.5 us
    all_gather x2, blocking collectives, gathered_once(): both, at, found = (lax.all_gather(jnp.concatenate(lines), axis), 0, {})  32.4 us
    all_to_all x2, blocking collectives, summed_on_arrival(): lax.all_to_all(in_blocks(shard, dim, peers), axis, 0, 0, tiled=True)  27.8 us
    dot_general x32, matrix products, advance(): jnp.einsum('qxe,qxt->qet', key_piece * jnp.exp(final_log_decay - decay_pi...  17.8 us
    dot_general x32, matrix products, advance(): block_result = jnp.einsum('hij,hjv->hiv', scores, value_piece)  15.6 us
    dot_general x32, matrix products, advance(): jnp.einsum('rus,rsp->rup', query_piece * jnp.exp(decay_piece), running_st...  14.1 us
  transfers between devices with their start and end apart: 2, of which 0 were waited for; matrix products, arithmetic and copies ran while one was open for 39% of the time, Pallas kernels for 0%

commit v1 on v0

v1 whole, which is shorter than its diff:
```python
import functools

import jax
import jax.numpy as jnp
from jax import lax
from jax.experimental import pallas as pl
from jax.experimental.pallas import tpu as pltpu
from jax.sharding import Mesh
from jax.sharding import PartitionSpec as P

SP = ("sp_0", "sp_1")
TP = ("tp_0", "tp_1")
SP_TP = ("sp_0", "sp_1", "tp_0", "tp_1")
EPS = 1e-06
MESH = pl.DeviceIdType.MESH
BF16, F32 = jnp.bfloat16, jnp.float32

NZ, NY, NX = 8, 4, 4
CH = 128
NCH = 8
KA, KB = 128, 64
FF = 768
WR = 192
XR = 80
XCUT = 48
YCUT = XR + 64
DT = (((1,), (1,)), ((), ()))
TD = (((0,), (0,)), ((), ()))


def dot(a, b):
    return jnp.dot(a, b, preferred_element_type=F32)


def dotg(a, b, dims):
    return lax.dot_general(a, b, dims, preferred_element_type=F32)


class Net:
    def __init__(self, ssem, rsem):
        self.ssem, self.rsem = ssem, rsem
        self.z, self.y = lax.axis_index("sp_0"), lax.axis_index("sp_1")
        self.x, self.c = lax.axis_index("tp_0"), lax.axis_index("tp_1")
        self.count = 0
        self.sent = []

    def number(self):
        self.count += 1
        return self.count - 1

    def at_z(self, k):
        return lax.rem(self.z + (k + NZ), NZ)

    def at_y(self, k):
        return lax.rem(self.y + (k + NY), NY)

    def at_x(self, k):
        return lax.rem(self.x + (k + NX), NX)

    def to_z(self, k):
        return (self.at_z(k), self.y, self.x, self.c)

    def to_y(self, k):
        return (self.z, self.at_y(k), self.x, self.c)

    def to_x(self, k):
        return (self.z, self.y, self.at_x(k), self.c)

    def partner(self):
        return (self.z, self.y, self.x, 1 - self.c)

    def _copy(self, src, dst, number, device):
        return pltpu.make_async_remote_copy(
            src_ref=src,
            dst_ref=dst,
            send_sem=self.ssem.at[number],
            recv_sem=self.rsem.at[number],
            device_id=device,
            device_id_type=MESH,
        )

    def send(self, src, dst, number, device):
        copy = self._copy(src, dst, number, device)
        copy.start()
        self.sent.append(copy)

    def arrived(self, dst, number):
        self._copy(dst, dst, number, self.partner()).wait_recv()

    def drain(self):
        for copy in self.sent:
            copy.wait_send()

    def greet(self):
        barrier = pltpu.get_barrier_semaphore()
        peers = [self.partner()]
        peers += [self.to_x(k) for k in (1, -1)]
        peers += [self.to_y(k) for k in range(1, NY)]
        peers += [self.to_z(k) for k in range(1, NZ)]
        for device in peers:
            pl.semaphore_signal(barrier, inc=1, device_id=device, device_id_type=MESH)
        pl.semaphore_wait(barrier, len(peers))


class Weights:
    def __init__(self, net, w, wg, lsem):
        self.net, self.w, self.wg, self.lsem = net, w, wg, lsem
        n = net.number
        self.xb = [n(), n()]
        self.xf = [n(), n()]
        self.xz = [[n(), n()] for _ in range(NZ // 2)]
        self.yz = [[n(), n()] for _ in range(NZ // 2)]
        self.yb = [[n(), n()] for _ in range(NZ)]
        self.yf = [[n(), n()] for _ in range(NZ)]

    def own(self):
        net = self.net
        self.local = pltpu.make_async_copy(self.w, self.wg.at[net.z, net.y], self.lsem)
        self.local.start()

    def own_done(self):
        self.local.wait()

    def x_slot(self, ky, lo, hi):
        return self.wg.at[self.net.z, self.net.at_y(ky), lo:hi]

    def x_out(self):
        net = self.net
        for d, k in enumerate((1, -1)):
            net.send(self.w.at[0:XR], self.x_slot(0, 0, XR), self.xb[d], net.to_y(k))

    def x_forward(self):
        net = self.net
        for d, (k, lo, hi) in enumerate(((1, 0, XCUT), (-1, XCUT, XR))):
            net.arrived(self.x_slot(-k, 0, XR), self.xb[d])
            part = self.x_slot(-k, lo, hi)
            net.send(part, part, self.xf[d], net.to_y(k))

    def x_forwarded(self):
        for d, (lo, hi) in enumerate(((0, XCUT), (XCUT, XR))):
            self.net.arrived(self.x_slot(2, lo, hi), self.xf[d])

    def x_bundle(self, kz, s, d):
        lo, hi = (0, NY) if s < NZ // 2 else ((0, NY // 2) if d == 0 else (NY // 2, NY))
        return self.wg.at[self.net.at_z(kz), lo:hi, 0:XR]

    def xz_send(self, s):
        for d, k in enumerate((1, -1)):
            part = self.x_bundle(-k * (s - 1), s, d)
            self.net.send(part, part, self.xz[s - 1][d], self.net.to_z(k))

    def xz_wait(self, s):
        for d, k in enumerate((1, -1)):
            self.net.arrived(self.x_bundle(-k * s, s, d), self.xz[s - 1][d])

    def y_rows(self, s, d):
        return (XR, WR) if s < NZ // 2 else ((XR, YCUT) if d == 0 else (YCUT, WR))

    def y_slot(self, kz, lo, hi, ky=0):
        return self.wg.at[self.net.at_z(kz), self.net.at_y(ky), lo:hi]

    def yz_send(self, s):
        net = self.net
        for d, k in enumerate((1, -1)):
            lo, hi = self.y_rows(s, d)
            part = self.y_slot(-k * (s - 1), lo, hi)
            src = self.w.at[lo:hi] if s == 1 else part
            net.send(src, part, self.yz[s - 1][d], net.to_z(k))

    def yz_wait(self, s):
        for d, k in enumerate((1, -1)):
            lo, hi = self.y_rows(s, d)
            self.net.arrived(self.y_slot(-k * s, lo, hi), self.yz[s - 1][d])

    def yb_send(self, kz):
        net = self.net
        slot = self.y_slot(kz, XR, WR)
        src = self.w.at[XR:WR] if kz == 0 else slot
        for d, k in enumerate((1, -1)):
            net.send(src, slot, self.yb[kz % NZ][d], net.to_y(k))

    def yf_send(self, kz):
        net = self.net
        for d, (k, lo, hi) in enumerate(((1, XR, YCUT), (-1, YCUT, WR))):
            net.arrived(self.y_slot(kz, XR, WR, -k), self.yb[kz % NZ][d])
            part = self.y_slot(kz, lo, hi, -k)
            net.send(part, part, self.yf[kz % NZ][d], net.to_y(k))

    def yf_wait(self, kz):
        for d, (lo, hi) in enumerate(((XR, YCUT), (YCUT, WR))):
            self.net.arrived(self.y_slot(kz, lo, hi, 2), self.yf[kz % NZ][d])


def rows_of(chunk, size=CH):
    return pl.ds(pl.multiple_of(chunk * size, size), size)


def iotas(n):
    return (
        lax.broadcasted_iota(jnp.int32, (n, n), 0),
        lax.broadcasted_iota(jnp.int32, (n, n), 1),
    )


class Attention:
    def __init__(self, net, r):
        self.net, self.r = net, r
        n = net.number
        self.m1 = [n() for _ in range(NY)]
        self.m2 = [n() for _ in range(NZ)]
        self.m3 = [n() for _ in range(NY)]
        self.heads = (
            (KA, r["qa"], r["ka"], r["ga"], r["ba"], r["sa"], r["ea"], r["pa"], r["ta"], 0),
            (KB, r["qb"], r["kb"], r["gb"], r["bb"], r["sb"], r["eb"], r["pb"], r["tb"], 1),
        )

    def states(self):
        r = self.r
        row, col = iotas(CH)
        lower = row >= col
        tri = jnp.where(lower, 1.0, 0.0).astype(BF16)
        tri2 = jnp.concatenate([tri, tri], axis=1)

        def step(c, carry):
            rows = rows_of(c)
            line = r["fade"][pl.ds(c, 1), :]
            fade = jnp.sum(jnp.where(lower, line, 0.0), axis=1, keepdims=True)
            new = []
            for (width, q, k, g, b, s, e, p, t, h), (state, before) in zip(self.heads, carry):
                x = g[rows, :].astype(F32)
                slow = (jnp.minimum(x, 0.0) - jnp.log1p(jnp.exp(-jnp.abs(x)))) * (1.0 / 16.0)
                high = slow.astype(BF16)
                low = (slow - high.astype(F32)).astype(BF16)
                sums = dot(tri2, jnp.concatenate([high, low], axis=0)) + fade
                b[rows, :] = sums
                total = sums[CH - 1 : CH, :]
                faded = (k[rows, :].astype(F32) * jnp.exp(total - sums)).astype(BF16)
                s[c] = state
                e[pl.ds(c, 1), :] = before
                state = jnp.exp(total) * state + dotg(r["v"][h, rows, :], faded, TD)
                new.append((state, before + total))
            return tuple(new)

        zero = tuple(
            (jnp.zeros((CH, width), F32), jnp.zeros((1, width), F32)) for width in (KA, KB)
        )
        (state_a, log_a), (state_b, log_b) = lax.fori_loop(0, NCH, step, zero)
        out = r["m1s"]
        quarter = CH // NY
        row16 = lax.broadcasted_iota(jnp.int32, (16, 1), 0)

        def two_rows(value):
            high = value.astype(BF16).astype(F32)
            return jnp.where(row16 == 0, high, value - high).astype(BF16)

        ends_a, ends_b = two_rows(jnp.exp(log_a)), two_rows(jnp.exp(log_b))
        for i in range(NY):
            part = slice(i * quarter, (i + 1) * quarter)
            out[i, 0:quarter, 0:KA] = state_a[part].astype(BF16)
            out[i, 0:quarter, KA : KA + KB] = state_b[part].astype(BF16)
            out[i, 0:quarter, KA + KB :] = jnp.zeros((quarter, KB), BF16)
            out[i, quarter:, 0:KA] = ends_a
            out[i, quarter:, KA : KA + KB] = ends_b
            out[i, quarter:, KA + KB :] = jnp.zeros((16, KB), BF16)

    def send_quarters(self):
        net, r = self.net, self.r
        for k in range(1, NY):
            net.send(r["m1s"].at[net.at_y(k)], r["m1r"].at[k], self.m1[k], net.to_y(k))

    @staticmethod
    def opened(message):
        quarter = CH // NY
        state = message[0:quarter, :].astype(F32)
        decay = message[quarter : quarter + 1, :].astype(F32) + message[
            quarter + 1 : quarter + 2, :
        ].astype(F32)
        return state, decay

    def send_line_total(self):
        net, r = self.net, self.r
        quarter = CH // NY
        for k in range(1, NY):
            net.arrived(r["m1r"].at[k], self.m1[k])
        r["m1r"][0] = r["m1s"][net.y]
        state = jnp.zeros((quarter, 256), F32)
        decay = jnp.ones((1, 256), F32)
        for i in range(NY):
            slot = lax.rem(net.y - i + NY, NY)
            own, factor = self.opened(r["m1r"][slot])
            state, decay = factor * state + own, factor * decay
        row16 = lax.broadcasted_iota(jnp.int32, (16, 1), 0)
        high = decay.astype(BF16).astype(F32)
        r["m2s"][0:quarter, :] = state.astype(BF16)
        r["m2s"][quarter:, :] = jnp.where(row16 == 0, high, decay - high).astype(BF16)
        for k in (1, -1, 2, -2, 3, -3, 4):
            net.send(r["m2s"], r["m2r"].at[k % NZ], self.m2[k % NZ], net.to_z(k))

    def send_incoming(self):
        net, r = self.net, self.r
        quarter = CH // NY
        for k in range(1, NZ):
            net.arrived(r["m2r"].at[k], self.m2[k])
        r["m2r"][0] = jnp.zeros((48, 256), BF16)
        state = jnp.zeros((quarter, 256), F32)
        for i in range(NZ - 1):
            slot = lax.rem(net.z - i + NZ, NZ)
            own, factor = self.opened(r["m2r"][slot])
            state = jnp.where(i < net.z, factor * state + own, state)
        for i in range(NY):
            r["m3s"][i] = state.astype(BF16)
            slot = lax.rem(net.y - i + NY, NY)
            own, factor = self.opened(r["m1r"][slot])
            state = factor * state + own
        for k in range(1, NY):
            net.send(r["m3s"].at[net.at_y(k)], r["m3r"].at[net.y], self.m3[k], net.to_y(k))
        r["m3r"][net.y] = r["m3s"][net.y]

    def incoming(self):
        net, r = self.net, self.r
        for k in range(1, NY):
            net.arrived(r["m3r"].at[net.at_y(-k)], self.m3[k])

    def scores(self, start, stop):
        r = self.r
        row, col = iotas(CH)
        near = ((row >> 5) == (col >> 5)) & (row >= col)
        middle = ((row >> 6) == (col >> 6)) & ((row >> 5) > (col >> 5))
        far = (row >> 6) > (col >> 6)

        def around(sums, size, at):
            width = sums.shape[1]
            parts = sums.reshape(CH // size, size, width)
            return (parts - parts[:, at : at + 1, :]).reshape(CH, width)

        def step(c, carry):
            rows = rows_of(c)
            for width, q, k, g, b, s, e, p, t, h in self.heads:
                sums = b[rows, :]
                query = q[rows, :].astype(F32) * (width**-0.5)
                key = k[rows, :].astype(F32)
                t[rows, :] = (query * jnp.exp(sums)).astype(BF16)
                at = around(sums, 32, 15)
                local = dotg(
                    (query * jnp.exp(at)).astype(BF16), (key * jnp.exp(-at)).astype(BF16), DT
                )
                total = jnp.where(near, local, 0.0)
                for size, at, mask in ((64, 31, middle), (128, 63, far)):
                    f = jnp.exp(-jnp.abs(around(sums, size, at)))
                    wide = dotg((query * f).astype(BF16), (key * f).astype(BF16), DT)
                    total = jnp.where(mask, wide, total)
                p[c] = total.astype(BF16)
            return carry

        lax.fori_loop(start, stop, step, 0)

    def gated(self, first, count):
        r = self.r

        def step(i, carry):
            c = first + i
            rows = rows_of(c)
            before_state = r["m3r"][...].astype(F32).reshape(CH, 256)
            for width, q, k, g, b, s, e, p, t, h in self.heads:
                state = s[c] + jnp.exp(e[pl.ds(c, 1), :]) * before_state[:, h * KA : h * KA + width]
                out = dot(p[c], r["v"][h, rows, :]) + dotg(t[rows, :], state.astype(BF16), DT)
                inverse = lax.rsqrt(jnp.mean(out * out, axis=-1, keepdims=True) + EPS)
                gate = r["og"][h, rows, :].astype(F32)
                normed = out * inverse * r["gain"][h : h + 1, :]
                value = gate * jax.nn.sigmoid(gate) * normed
                r["gat"][rows, h * CH : (h + 1) * CH] = value.astype(BF16)
            return carry

        lax.fori_loop(0, count, step, 0)


HALF = 1024
BLK = 256
LEFT, RIGHT = slice(0, 512), slice(512, 1024)


class Reduce:
    def __init__(self, net, part, comb, hop, joined, direct):
        self.net, self.part, self.comb = net, part, comb
        self.hop, self.joined, self.direct = hop, joined, direct
        n = net.number
        self.h = [[n(), n()] for _ in range(2)]
        self.j = [[n(), n()] for _ in range(2)]
        self.d = [n(), n()]

    def send_far(self):
        net = self.net
        for piece in range(2):
            rows = pl.ds(piece * CH, CH)
            for side, (k, cols) in enumerate(((1, LEFT), (-1, RIGHT))):
                net.send(
                    self.part.at[0, rows, cols],
                    self.hop.at[side, rows],
                    self.h[side][piece],
                    net.to_x(k),
                )

    def send_near(self):
        net = self.net
        for side, (k, block, cols) in enumerate(((1, 1, RIGHT), (-1, 2, LEFT))):
            net.send(
                self.part.at[block, :, cols], self.direct.at[side], self.d[side], net.to_x(k)
            )

    def join(self):
        net = self.net
        for piece in range(2):
            rows = slice(piece * CH, (piece + 1) * CH)
            for side, (k, block, cols) in enumerate(((1, 1, LEFT), (-1, 2, RIGHT))):
                net.arrived(self.hop.at[side, rows], self.h[side][piece])
                both = self.part[block, rows, cols].astype(F32) + self.hop[side, rows, :].astype(
                    F32
                )
                self.comb[side, rows, :] = both.astype(BF16)
                net.send(
                    self.comb.at[side, rows],
                    self.joined.at[side, rows],
                    self.j[side][piece],
                    net.to_x(k),
                )

    def arrived(self, piece):
        net = self.net
        rows = slice(piece * CH, (piece + 1) * CH)
        if piece == 0:
            for side in range(2):
                net.arrived(self.direct.at[side], self.d[side])
        for side in range(2):
            net.arrived(self.joined.at[side, rows], self.j[side][piece])

    def total(self, own, rows):
        left = (
            own[rows, LEFT]
            + self.joined[0, rows, :].astype(F32)
            + self.direct[1, rows, :].astype(F32)
        )
        right = (
            own[rows, RIGHT]
            + self.joined[1, rows, :].astype(F32)
            + self.direct[0, rows, :].astype(F32)
        )
        return left, right


class Feed:
    def __init__(self, net, r):
        self.net, self.r = net, r
        n = net.number
        self.n_res, self.n_wo, self.n_ss, self.n_out, self.n_dp = n(), n(), n(), n(), n()
        self.n_gat = [n() for _ in range(NX)]
        self.n_hid = [n() for _ in range(NX)]
        self.ring = [[n(), n()] for _ in range(2)]
        self.far = [n(), n()]
        self.over = [[n(), n()] for _ in range(NX)]
        self.first = Reduce(net, r["p1"], r["c1"], r["h1"], r["j1"], r["d1"])
        self.second = Reduce(net, r["p2"], r["c2"], r["h2"], r["j2"], r["d2"])

    def cols(self, core):
        return pl.ds(pl.multiple_of(core * HALF, HALF), HALF)

    def block(self, k):
        return rows_of(self.net.at_x(k), BLK)

    def swap_inputs(self):
        net, r = self.net, self.r
        other = 1 - net.c
        net.send(
            r["res"].at[:, self.cols(other)], r["resp"], self.n_res, net.partner()
        )
        net.send(r["wo"].at[:, :, self.cols(other)], r["wop"], self.n_wo, net.partner())

    def send_gated(self, k):
        net, r = self.net, self.r
        rows = self.block(k)
        net.send(r["gat"].at[rows], r["gatp"].at[rows], self.n_gat[k % NX], net.partner())

    def swapped_projection(self):
        self.net.arrived(self.r["wop"], self.n_wo)

    def project(self, k):
        net, r = self.net, self.r
        rows = self.block(k)
        net.arrived(r["gatp"].at[rows], self.n_gat[k % NX])
        mine, theirs = r["gat"][rows, :], r["gatp"][rows, :]
        for side in range(2):
            cols = slice(side * 512, (side + 1) * 512)
            at = pl.ds(pl.multiple_of(net.c * HALF + side * 512, 512), 512)
            part = dot(mine, r["wo"][:, :, at].reshape(2 * CH, 512)) + dot(
                theirs, r["wop"][:, :, cols].reshape(2 * CH, 512)
            )
            if k == 0:
                r["own1"][:, cols] = part
            else:
                r["p1"][{2: 0, 1: 1, -1: 2}[k], :, cols] = part.astype(BF16)

    def middle(self):
        net, r = self.net, self.r
        net.arrived(r["resp"], self.n_res)
        for piece in range(2):
            self.first.arrived(piece)
            rows = slice(piece * CH, (piece + 1) * CH)
            left, right = self.first.total(r["own1"], rows)
            mine = r["res"][:, self.cols(net.c)]
            theirs = r["resp"][...]
            base = jnp.where(net.c == piece, mine.astype(F32), theirs.astype(F32))
            mid_l = (base[:, LEFT] + left).astype(BF16)
            mid_r = (base[:, RIGHT] + right).astype(BF16)
            r["mid"][rows, LEFT] = mid_l
            r["mid"][rows, RIGHT] = mid_r
            mid_l, mid_r = mid_l.astype(F32), mid_r.astype(F32)
            squares = jnp.sum(mid_l * mid_l, axis=-1, keepdims=True) + jnp.sum(
                mid_r * mid_r, axis=-1, keepdims=True
            )
            r["ss"][rows, :] = jnp.broadcast_to(squares, (CH, 128))
        net.send(r["ss"], r["ssp"], self.n_ss, net.partner())
        net.arrived(r["ssp"], self.n_ss)
        inverse = lax.rsqrt((r["ss"][...] + r["ssp"][...])[:, 0:1] * (1.0 / 2048.0) + EPS)
        gain = r["fgain"][:, self.cols(net.c)]
        normed = (r["mid"][...].astype(F32) * inverse * gain).astype(BF16)
        r["all"][net.c, self.block(0), :] = normed

    def piece(self, k, half):
        start = self.net.at_x(k) * BLK + half * CH
        return self.r["all"].at[self.net.c, pl.ds(pl.multiple_of(start, CH), CH)]

    def over_send(self, k, half):
        part = self.piece(k, half)
        self.net.send(part, part, self.over[k % NX][half], self.net.partner())

    def over_wait(self, k):
        for half in range(2):
            start = self.net.at_x(k) * BLK + half * CH
            dst = self.r["all"].at[1 - self.net.c, pl.ds(pl.multiple_of(start, CH), CH)]
            self.net.arrived(dst, self.over[k % NX][half])

    def rows_out(self):
        net = self.net
        for order in range(2):
            for d, k in enumerate((1, -1)):
                half = order if d == 0 else 1 - order
                part = self.piece(0, half)
                net.send(part, part, self.ring[d][half], net.to_x(k))
            self.over_send(0, order)

    def rows_on(self):
        net = self.net
        for d, (k, half) in enumerate(((1, 0), (-1, 1))):
            part = self.piece(-k, half)
            net.arrived(part, self.ring[d][half])
            net.send(part, part, self.far[d], net.to_x(k))
            self.over_send(-k, half)

    def rows_rest(self):
        net = self.net
        for d, (k, half) in enumerate(((1, 1), (-1, 0))):
            net.arrived(self.piece(-k, half), self.ring[d][half])
            self.over_send(-k, half)

    def rows_far(self):
        for d, half in enumerate((0, 1)):
            self.net.arrived(self.piece(2, half), self.far[d])
            self.over_send(2, half)

    def hidden(self, k):
        net, r = self.net, self.r
        rows = self.block(k)

        def step(n, carry):
            at = pl.ds(pl.multiple_of(n * 256, 256), 256)
            sums = []
            for low in (0, 128):
                total = None
                for half in range(2):
                    w = r["wg"][half * 4 : half * 4 + 4, :, low : low + 64, at]
                    part = dot(r["all"][half, rows, :], w.reshape(HALF, 256))
                    total = part if total is None else total + part
                sums.append(total)
            gate, up = sums
            r["hid"][rows, at] = (gate * jax.nn.sigmoid(gate) * up).astype(BF16)
            return carry

        lax.fori_loop(0, FF // 256, step, 0)
        net.send(r["hid"].at[rows], r["hidp"].at[rows], self.n_hid[k % NX], net.partner())

    def swap_down(self):
        net, r = self.net, self.r
        part = r["wg"].at[pl.ds(4 * (1 - net.c), 4), :, 64:128, :]
        net.send(part, r["dp"], self.n_dp, net.partner())

    def swapped_down(self):
        self.net.arrived(self.r["dp"], self.n_dp)

    def down(self, k):
        net, r = self.net, self.r
        rows = self.block(k)
        net.arrived(r["hidp"].at[rows], self.n_hid[k % NX])

        def step(n, carry):
            at = pl.ds(pl.multiple_of(n * 256, 256), 256)
            w = r["wg"][4 * net.c + n, :, 64:128, :].reshape(256, FF)
            part = dotg(r["hid"][rows, :], w, DT) + dotg(
                r["hidp"][rows, :], r["dp"][n].reshape(256, FF), DT
            )
            if k == 0:
                r["own2"][:, at] = part
            else:
                r["p2"][{2: 0, 1: 1, -1: 2}[k], :, at] = part.astype(BF16)
            return carry

        lax.fori_loop(0, HALF // 256, step, 0)

    def finish(self):
        net, r = self.net, self.r
        for piece in range(2):
            self.second.arrived(piece)
            rows = slice(piece * CH, (piece + 1) * CH)
            left, right = self.second.total(r["own2"], rows)
            r["outs"][piece, :, LEFT] = (r["mid"][rows, LEFT].astype(F32) + left).astype(BF16)
            r["outs"][piece, :, RIGHT] = (r["mid"][rows, RIGHT].astype(F32) + right).astype(BF16)
        net.send(r["outs"].at[1 - net.c], r["outp"], self.n_out, net.partner())
        r["out"][:, self.cols(net.c)] = r["outs"][net.c]
        net.arrived(r["outp"], self.n_out)
        r["out"][:, self.cols(1 - net.c)] = r["outp"][...]


INPUTS = ["res", "qa", "ka", "qb", "kb", "ga", "gb", "fade", "v", "og", "gain", "wo", "fgain", "w"]
SCRATCH = dict(
    wg=((NZ, NY, WR, FF), BF16),
    ba=((1024, KA), F32),
    bb=((1024, KB), F32),
    sa=((NCH, CH, KA), F32),
    sb=((NCH, CH, KB), F32),
    ea=((NCH, KA), F32),
    eb=((NCH, KB), F32),
    pa=((NCH, CH, CH), BF16),
    pb=((NCH, CH, CH), BF16),
    ta=((1024, KA), BF16),
    tb=((1024, KB), BF16),
    m1s=((NY, 48, 256), BF16),
    m1r=((NY, 48, 256), BF16),
    m2s=((48, 256), BF16),
    m2r=((NZ, 48, 256), BF16),
    m3s=((NY, 32, 256), BF16),
    m3r=((NY, 32, 256), BF16),
    gat=((1024, 256), BF16),
    gatp=((1024, 256), BF16),
    wop=((2, CH, HALF), BF16),
    resp=((CH, HALF), BF16),
    own1=((BLK, HALF), F32),
    p1=((3, BLK, HALF), BF16),
    c1=((2, BLK, 512), BF16),
    h1=((2, BLK, 512), BF16),
    j1=((2, BLK, 512), BF16),
    d1=((2, BLK, 512), BF16),
    mid=((BLK, HALF), BF16),
    ss=((BLK, 128), F32),
    ssp=((BLK, 128), F32),
    all=((2, 1024, HALF), BF16),
    hid=((1024, FF), BF16),
    hidp=((1024, FF), BF16),
    dp=((4, NY, 64, FF), BF16),
    own2=((BLK, HALF), F32),
    p2=((3, BLK, HALF), BF16),
    c2=((2, BLK, 512), BF16),
    h2=((2, BLK, 512), BF16),
    j2=((2, BLK, 512), BF16),
    d2=((2, BLK, 512), BF16),
    outs=((2, CH, HALF), BF16),
    outp=((CH, HALF), BF16),
)
COPIES = 128


def kernel(*refs):
    names = INPUTS + ["out"] + list(SCRATCH)
    r = dict(zip(names, refs))
    lsem, ssem, rsem = refs[len(names) :]
    net = Net(ssem, rsem)
    weights = Weights(net, r["w"], r["wg"], lsem)
    attention = Attention(net, r)
    feed = Feed(net, r)
    assert net.count <= COPIES, net.count
    net.greet()
    weights.own()
    weights.x_out()
    weights.yz_send(1)
    feed.swap_inputs()
    attention.states()
    attention.send_quarters()
    weights.x_forward()
    weights.yz_wait(1)
    weights.yz_send(2)
    weights.yb_send(0)
    attention.scores(0, 3)
    attention.send_line_total()
    attention.scores(3, 8)
    weights.own_done()
    weights.yz_wait(2)
    weights.yz_send(3)
    attention.send_incoming()
    weights.x_forwarded()
    weights.xz_send(1)
    for k in (1, -1, 2, -2):
        weights.yb_send(k)
    weights.yz_wait(3)
    weights.yz_send(4)
    attention.incoming()
    feed.swapped_projection()
    for k in (2, 1, -1, 0):
        attention.gated(2 * net.at_x(k), 2)
        feed.send_gated(k)
        if k == 1:
            feed.project(2)
            feed.first.send_far()
    feed.project(1)
    feed.project(-1)
    feed.first.send_near()
    feed.project(0)
    weights.yf_send(0)
    weights.yz_wait(4)
    for k in (3, -3, 4):
        weights.yb_send(k)
    weights.xz_wait(1)
    weights.xz_send(2)
    feed.first.join()
    weights.yf_send(1)
    weights.yf_send(-1)
    weights.xz_wait(2)
    weights.xz_send(3)
    feed.middle()
    feed.rows_out()
    weights.yf_send(2)
    weights.yf_send(-2)
    weights.xz_wait(3)
    weights.xz_send(4)
    feed.rows_on()
    weights.yf_send(3)
    weights.yf_send(-3)
    weights.yf_send(4)
    for k in (0, 1, -1, 2, -2, 3, -3, 4):
        weights.yf_wait(k)
    weights.xz_wait(4)
    feed.swap_down()
    feed.over_wait(0)
    feed.hidden(0)
    feed.rows_rest()
    feed.over_wait(1)
    feed.hidden(1)
    feed.over_wait(-1)
    feed.hidden(-1)
    feed.swapped_down()
    feed.down(1)
    feed.down(-1)
    feed.second.send_near()
    feed.rows_far()
    feed.over_wait(2)
    feed.hidden(2)
    feed.down(2)
    feed.second.send_far()
    feed.down(0)
    feed.second.join()
    feed.finish()
    net.drain()


def per_device(
    residual,
    first_group_queries,
    first_group_keys,
    second_group_queries,
    second_group_keys,
    primary_retain_switch_inputs,
    secondary_retain_switch_inputs,
    timestep_fading_exponent,
    values,
    output_gate_logits,
    head_norm_gains,
    output_projection,
    feedforward_norm_gain,
    gate_projection,
    up_projection,
    down_projection,
):
    w = jnp.concatenate([gate_projection, down_projection.T, up_projection], axis=0)
    args = (
        residual,
        first_group_queries,
        first_group_keys,
        second_group_queries,
        second_group_keys,
        primary_retain_switch_inputs,
        secondary_retain_switch_inputs,
        timestep_fading_exponent.reshape(NCH, CH),
        values,
        output_gate_logits,
        head_norm_gains,
        output_projection,
        feedforward_norm_gain.reshape(1, -1),
        w,
    )
    return pl.pallas_call(
        kernel,
        out_shape=jax.ShapeDtypeStruct(residual.shape, BF16),
        in_specs=[pl.BlockSpec(memory_space=pltpu.VMEM)] * len(args),
        out_specs=pl.BlockSpec(memory_space=pltpu.VMEM),
        scratch_shapes=[pltpu.VMEM(shape, dtype) for shape, dtype in SCRATCH.values()]
        + [
            pltpu.SemaphoreType.DMA,
            pltpu.SemaphoreType.DMA((COPIES,)),
            pltpu.SemaphoreType.DMA((COPIES,)),
        ],
        compiler_params=pltpu.CompilerParams(
            collective_id=0, has_side_effects=True, vmem_limit_bytes=66000000
        ),
    )(*args)


def solution(mesh):
    finer = Mesh(mesh.devices.reshape(NZ, NY, NX, 2), SP_TP)
    return jax.shard_map(
        per_device,
        mesh=finer,
        in_specs=(
            P(SP_TP, None),
            P(SP, TP),
            P(SP, TP),
            P(SP, TP),
            P(SP, TP),
            P(SP, TP),
            P(SP, TP),
            P(SP),
            P(None, SP, TP),
            P(None, SP, TP),
            P(None, TP),
            P(None, TP, None),
            P(),
            P(SP, TP),
            P(SP, TP),
            P(TP, SP),
        ),
        out_specs=P(SP_TP, None),
        check_vma=False,
    )
```

time: 341 us -> 119 us (0.35)
  blocking collectives: 168 us -> 0 us
  Pallas kernels: 0 us -> 112 us
  matrix products: 75.1 us -> 0 us
  other arithmetic: 65.8 us -> 0.73 us
  between operations: 13.9 us -> 0.02 us
  local copies, waits for them, and re-layouts: 13.2 us -> 5.54 us
    all_to_all x6 -> x0, blocking collectives: 122 us -> none  [the longest x2 58 us: summed_rows(): lax.all_to_all(own.astype(jnp.bfloat16), far, 0, 0, tiled=True)]
    pallas_call x0 -> x1, Pallas kernels: none -> 112 us  [per_device(): pl.pallas_call(kernel, out_shape=jax.ShapeDtypeStruct(residual.shape, BF1...]
    dot_general x102 -> x0, matrix products: 75.1 us -> none  [the longest x32 17.8 us: advance(): jnp.einsum('qxe,qxt->qet', key_piece * jnp.exp(final_log_decay - decay_pi...]
    reduce_sum x38 -> x0, other arithmetic: 51.2 us -> none  [the longest x32 43.1 us: advance(): jnp.sum(query_piece[:, :, None, :] * key_piece[:, None, :, :] * decay_gri...]
    all_gather x3 -> x0, blocking collectives: 45.5 us -> none  [the longest x2 32.4 us: gathered_once(): both, at, found = (lax.all_gather(jnp.concatenate(lines), axis), 0, {})]
    another operation x5 -> x0, other arithmetic: 7.67 us -> none  [the longest x2 6.64 us: within_block_pass(): jnp.cumsum(blocks(decay_logarithm, block_count, head_count, key_width), a...]
    another operation x10 -> x0, local copies, waits for them, and re-layouts: 5.03 us -> none  [the longest x2 2.8 us: in_blocks(): shard.reshape(*dims[:dim], peers, dims[dim] // peers, *dims[dim + 1:])]
    unnamed x27 -> x14, local copies, waits for them, and re-layouts: 1.07 us -> 5.54 us
  transfers between devices with their start and end apart: 2 -> 0, of which waited for: 0 -> 0; matrix products, arithmetic and copies ran while one was open for 39% -> 0% of each run, Pallas kernels for 0% -> 0%
where the time goes in v1:
time: 119 us
  Pallas kernels  112 us (94%)
  local copies, waits for them, and re-layouts  5.54 us (5%)
    pallas_call x1, Pallas kernels, per_device(): pl.pallas_call(kernel, out_shape=jax.ShapeDtypeStruct(residual.shape, BF1...  112 us
    unnamed x14, local copies, waits for them, and re-layouts  5.54 us

profile of v1, /device:TPU:1, one launch (start us, length us, event | category | flops | bytes accessed | tf_op | source)
XLA Modules:
  0.0 118.6 jit_solution(1676082944488958383)
XLA Ops:
  0.0 0.0 copy-start
  0.0 1.8 %copy.17.refs_3_ = bf16[1024,64]{1,0:T(8,128)(2,1)} copy(bf16[1024,64]{0,1:T(8,128)(2,1)} %param.19) | data formatting | bytes 262144 | tf_op args[3]
  1.8 0.0 copy-done
  1.8 0.0 copy-start.1
  1.8 0.8 copy.18.refs_4_
  2.6 0.1 copy-done.1
  2.7 0.0 copy-start.2
  2.7 0.0 copy-start.3
  2.7 0.0 copy-start.4
  2.7 0.8 copy.19.refs_6_
  3.5 0.1 copy-done.2
  3.6 0.0 copy-done.3
  3.6 0.0 copy-done.4
  3.7 0.7 pad_maximum_fusion.refs_13_
  4.4 112.4 %shard_map.154 = bf16[128,2048]{1,0:T(8,128)(2,1)} custom-call(bf16[128,2048]{1,0:T(8,128)(2,1)} %refs_0_.1, bf16[1024,128]{1,0:T(8,128)(2,1)} %refs_1_.1, bf16[1024,128]{1,0:T(8,128)(2,1)} %refs_2_.1, bf16[1024,64]{1,0:T(8,128)(2,1)} %copy.17.refs_3_, bf16[1024,64]{1,0:T(8,128)(2,1)} %copy.18.refs_4_, bf16[1024,128]{1,0:T(8,128)(2,1)} %refs_5_.1, ...), custom_call_target="tpu_custom_call" | custom-call | tf_op jit(solution)/shard_map/pallas_call | solution.py:806
  116.8 1.9 %copy.21 = bf16[128,2048]{1,0:T(8,128)(2,1)} copy(bf16[128,2048]{1,0:T(8,128)(2,1)} %shard_map.154) | data formatting | bytes 1048576
Async XLA Ops:
  0.0 1.8 %copy-start = (bf16[1024,64]{0,1:T(8,128)(2,1)S(1)}, bf16[1024,64]{0,1:T(8,128)(2,1)}, u32[]{:S(2)}) copy-start(bf16[1024,64]{0,1:T(8,128)(2,1)} %param.20) | copy-start | bytes 393220
  1.8 0.9 copy-start.1
  2.7 0.9 copy-start.2
  2.7 0.9 copy-start.3
  2.7 1.0 copy-start.4

commit v2 on v1

v2 whole, which is shorter than its diff:
```python
import functools

import jax
import jax.numpy as jnp
from jax import lax
from jax.experimental import pallas as pl
from jax.experimental.pallas import tpu as pltpu
from jax.sharding import Mesh
from jax.sharding import PartitionSpec as P

SP = ("sp_0", "sp_1")
TP = ("tp_0", "tp_1")
SP_TP = ("sp_0", "sp_1", "tp_0", "tp_1")
EPS = 1e-06
MESH = pl.DeviceIdType.MESH
BF16, F32 = jnp.bfloat16, jnp.float32

NZ, NY, NX = 8, 4, 4
CH = 128
NCH = 8
KA, KB = 128, 64
FF = 768
WR = 192
UP, DOWN = 64, 128
DT = (((1,), (1,)), ((), ()))
TD = (((0,), (0,)), ((), ()))


def dot(a, b):
    return jnp.dot(a, b, preferred_element_type=F32)


def dotg(a, b, dims):
    return lax.dot_general(a, b, dims, preferred_element_type=F32)


class Net:
    def __init__(self, ssem, rsem):
        self.ssem, self.rsem = ssem, rsem
        self.z, self.y = lax.axis_index("sp_0"), lax.axis_index("sp_1")
        self.x, self.c = lax.axis_index("tp_0"), lax.axis_index("tp_1")
        self.count = 0
        self.sent = []

    def number(self):
        self.count += 1
        return self.count - 1

    def at_z(self, k):
        return lax.rem(self.z + (k + NZ), NZ)

    def at_y(self, k):
        return lax.rem(self.y + (k + NY), NY)

    def at_x(self, k):
        return lax.rem(self.x + (k + NX), NX)

    def to_z(self, k):
        return (self.at_z(k), self.y, self.x, self.c)

    def to_y(self, k):
        return (self.z, self.at_y(k), self.x, self.c)

    def to_x(self, k):
        return (self.z, self.y, self.at_x(k), self.c)

    def partner(self):
        return (self.z, self.y, self.x, 1 - self.c)

    def _copy(self, src, dst, number, device):
        return pltpu.make_async_remote_copy(
            src_ref=src,
            dst_ref=dst,
            send_sem=self.ssem.at[number],
            recv_sem=self.rsem.at[number],
            device_id=device,
            device_id_type=MESH,
        )

    def send(self, src, dst, number, device):
        copy = self._copy(src, dst, number, device)
        copy.start()
        self.sent.append(copy)

    def arrived(self, dst, number):
        self._copy(dst, dst, number, self.partner()).wait_recv()

    def drain(self):
        for copy in self.sent:
            copy.wait_send()

    def greet(self):
        peers = [self.to_z(k) for k in (4, 3, -3, 2, -2, 1, -1)]
        peers += [self.to_y(k) for k in (2, 1, -1)]
        peers += [self.to_x(k) for k in (1, -1)]
        peers += [self.partner()]
        self.peers = len(peers)
        barrier = pltpu.get_barrier_semaphore()
        for device in peers:
            pl.semaphore_signal(barrier, inc=1, device_id=device, device_id_type=MESH)

    def greeted(self):
        pl.semaphore_wait(pltpu.get_barrier_semaphore(), self.peers)


class Weights:
    def __init__(self, net, wg):
        self.net, self.wg = net, wg
        n = net.number
        self.xb = [n(), n()]
        self.xf = [n(), n()]
        self.xz = [[n(), n()] for _ in range(NZ // 2)]
        self.yz = [[n(), n()] for _ in range(NZ // 2)]
        self.yb = {u: [[n(), n()] for _ in range(NZ)] for u in (UP, DOWN)}
        self.yf = {u: [[n(), n()] for _ in range(NZ)] for u in (UP, DOWN)}

    def slot(self, kz, ky, lo, hi):
        return self.wg.at[self.net.at_z(kz), self.net.at_y(ky), lo:hi]

    def x_out(self):
        net = self.net
        for d, k in enumerate((1, -1)):
            part = self.slot(0, 0, 0, 64)
            net.send(part, part, self.xb[d], net.to_y(k))

    def x_forward(self):
        net = self.net
        for d, (k, lo, hi) in enumerate(((1, 0, 32), (-1, 32, 64))):
            net.arrived(self.slot(0, -k, 0, 64), self.xb[d])
            part = self.slot(0, -k, lo, hi)
            net.send(part, part, self.xf[d], net.to_y(k))

    def x_forwarded(self):
        for d, (lo, hi) in enumerate(((0, 32), (32, 64))):
            self.net.arrived(self.slot(0, 2, lo, hi), self.xf[d])

    def x_bundle(self, kz, s, d):
        lo, hi = (0, NY) if s < NZ // 2 else ((0, NY // 2) if d == 0 else (NY // 2, NY))
        return self.wg.at[self.net.at_z(kz), lo:hi, 0:64]

    def xz_send(self, s):
        for d, k in enumerate((1, -1)):
            part = self.x_bundle(-k * (s - 1), s, d)
            self.net.send(part, part, self.xz[s - 1][d], self.net.to_z(k))

    def xz_wait(self, s):
        for d, k in enumerate((1, -1)):
            self.net.arrived(self.x_bundle(-k * s, s, d), self.xz[s - 1][d])

    def y_rows(self, s, d):
        return (64, 192) if s < NZ // 2 else ((64, 128) if d == 0 else (128, 192))

    def yz_send(self, s):
        net = self.net
        for d, k in enumerate((1, -1)):
            part = self.slot(-k * (s - 1), 0, *self.y_rows(s, d))
            net.send(part, part, self.yz[s - 1][d], net.to_z(k))

    def yz_wait(self, s):
        for d, k in enumerate((1, -1)):
            self.net.arrived(self.slot(-k * s, 0, *self.y_rows(s, d)), self.yz[s - 1][d])

    def yb_send(self, lo, *kzs):
        net = self.net
        for kz in kzs:
            part = self.slot(kz, 0, lo, lo + 64)
            for d, k in enumerate((1, -1)):
                net.send(part, part, self.yb[lo][kz % NZ][d], net.to_y(k))

    def yf_send(self, lo, *kzs):
        net = self.net
        for kz in kzs:
            for d, k in enumerate((1, -1)):
                net.arrived(self.slot(kz, -k, lo, lo + 64), self.yb[lo][kz % NZ][d])
                part = self.slot(kz, -k, lo + 32 * d, lo + 32 * d + 32)
                net.send(part, part, self.yf[lo][kz % NZ][d], net.to_y(k))

    def yf_wait(self, lo, *kzs):
        for kz in kzs:
            for d in range(2):
                part = self.slot(kz, 2, lo + 32 * d, lo + 32 * d + 32)
                self.net.arrived(part, self.yf[lo][kz % NZ][d])


def rows_of(chunk, size=CH):
    return pl.ds(pl.multiple_of(chunk * size, size), size)


def iotas(n):
    return (
        lax.broadcasted_iota(jnp.int32, (n, n), 0),
        lax.broadcasted_iota(jnp.int32, (n, n), 1),
    )


class Attention:
    def __init__(self, net, r):
        self.net, self.r = net, r
        n = net.number
        self.m1 = [n() for _ in range(NY)]
        self.m2 = [n() for _ in range(NZ)]
        self.m3 = [n() for _ in range(NY)]
        self.heads = (
            (KA, r["ba"], r["sa"], r["ea"], r["pa"], r["ta"], 0),
            (KB, r["bb"], r["sb"], r["eb"], r["pb"], r["tb"], 1),
        )

    def load(self, kind, h, rows):
        if h == 0:
            return self.r[kind + "a"][rows, :].astype(F32)
        return self.r[kind + "b"][:, rows].astype(F32).T

    def states(self):
        r = self.r
        row, col = iotas(CH)
        lower = row >= col
        tri = jnp.where(lower, 1.0, 0.0).astype(BF16)
        tri2 = jnp.concatenate([tri, tri], axis=1)

        def step(c, carry):
            rows = rows_of(c)
            line = r["fade"][pl.ds(c, 1), :]
            fade = jnp.sum(jnp.where(lower, line, 0.0), axis=1, keepdims=True)
            new = []
            for (width, b, s, e, p, t, h), (state, before) in zip(self.heads, carry):
                x = self.load("g", h, rows)
                slow = (jnp.minimum(x, 0.0) - jnp.log1p(jnp.exp(-jnp.abs(x)))) * (1.0 / 16.0)
                high = slow.astype(BF16)
                low = (slow - high.astype(F32)).astype(BF16)
                sums = dot(tri2, jnp.concatenate([high, low], axis=0)) + fade
                b[rows, :] = sums
                total = sums[CH - 1 : CH, :]
                faded = (self.load("k", h, rows) * jnp.exp(total - sums)).astype(BF16)
                s[c] = state
                e[pl.ds(c, 1), :] = before
                state = jnp.exp(total) * state + dotg(r["v"][h, rows, :], faded, TD)
                new.append((state, before + total))
            return tuple(new)

        zero = tuple(
            (jnp.zeros((CH, width), F32), jnp.zeros((1, width), F32)) for width in (KA, KB)
        )
        (state_a, log_a), (state_b, log_b) = lax.fori_loop(0, NCH, step, zero, unroll=4)
        out = r["m1s"]
        quarter = CH // NY
        row16 = lax.broadcasted_iota(jnp.int32, (16, 1), 0)

        def two_rows(value):
            high = value.astype(BF16).astype(F32)
            return jnp.where(row16 == 0, high, value - high).astype(BF16)

        ends_a, ends_b = two_rows(jnp.exp(log_a)), two_rows(jnp.exp(log_b))
        for i in range(NY):
            part = slice(i * quarter, (i + 1) * quarter)
            out[i, 0:quarter, 0:KA] = state_a[part].astype(BF16)
            out[i, 0:quarter, KA : KA + KB] = state_b[part].astype(BF16)
            out[i, 0:quarter, KA + KB :] = jnp.zeros((quarter, KB), BF16)
            out[i, quarter:, 0:KA] = ends_a
            out[i, quarter:, KA : KA + KB] = ends_b
            out[i, quarter:, KA + KB :] = jnp.zeros((16, KB), BF16)

    def send_quarters(self):
        net, r = self.net, self.r
        for k in range(1, NY):
            net.send(r["m1s"].at[net.at_y(k)], r["m1r"].at[k], self.m1[k], net.to_y(k))

    @staticmethod
    def opened(message):
        quarter = CH // NY
        state = message[0:quarter, :].astype(F32)
        decay = message[quarter : quarter + 1, :].astype(F32) + message[
            quarter + 1 : quarter + 2, :
        ].astype(F32)
        return state, decay

    def send_line_total(self):
        net, r = self.net, self.r
        quarter = CH // NY
        for k in range(1, NY):
            net.arrived(r["m1r"].at[k], self.m1[k])
        r["m1r"][0] = r["m1s"][net.y]
        state = jnp.zeros((quarter, 256), F32)
        decay = jnp.ones((1, 256), F32)
        for i in range(NY):
            slot = lax.rem(net.y - i + NY, NY)
            own, factor = self.opened(r["m1r"][slot])
            state, decay = factor * state + own, factor * decay
        row16 = lax.broadcasted_iota(jnp.int32, (16, 1), 0)
        high = decay.astype(BF16).astype(F32)
        r["m2s"][0:quarter, :] = state.astype(BF16)
        r["m2s"][quarter:, :] = jnp.where(row16 == 0, high, decay - high).astype(BF16)
        for k in (1, -1, 2, -2, 3, -3, 4):
            net.send(r["m2s"], r["m2r"].at[k % NZ], self.m2[k % NZ], net.to_z(k))

    def send_incoming(self):
        net, r = self.net, self.r
        quarter = CH // NY
        for k in range(1, NZ):
            net.arrived(r["m2r"].at[k], self.m2[k])
        r["m2r"][0] = jnp.zeros((48, 256), BF16)
        state = jnp.zeros((quarter, 256), F32)
        for i in range(NZ - 1):
            slot = lax.rem(net.z - i + NZ, NZ)
            own, factor = self.opened(r["m2r"][slot])
            state = jnp.where(i < net.z, factor * state + own, state)
        for i in range(NY):
            r["m3s"][i] = state.astype(BF16)
            slot = lax.rem(net.y - i + NY, NY)
            own, factor = self.opened(r["m1r"][slot])
            state = factor * state + own
        for k in range(1, NY):
            net.send(r["m3s"].at[net.at_y(k)], r["m3r"].at[net.y], self.m3[k], net.to_y(k))
        r["m3r"][net.y] = r["m3s"][net.y]

    def incoming(self):
        net, r = self.net, self.r
        for k in range(1, NY):
            net.arrived(r["m3r"].at[net.at_y(-k)], self.m3[k])

    def scores(self, start, stop):
        r = self.r
        row, col = iotas(CH)
        near = ((row >> 5) == (col >> 5)) & (row >= col)
        middle = ((row >> 6) == (col >> 6)) & ((row >> 5) > (col >> 5))
        far = (row >> 6) > (col >> 6)

        def around(sums, size, at):
            width = sums.shape[1]
            parts = sums.reshape(CH // size, size, width)
            return (parts - parts[:, at : at + 1, :]).reshape(CH, width)

        def step(c, carry):
            rows = rows_of(c)
            for width, b, s, e, p, t, h in self.heads:
                sums = b[rows, :]
                query = self.load("q", h, rows) * (width**-0.5)
                key = self.load("k", h, rows)
                t[rows, :] = (query * jnp.exp(sums)).astype(BF16)
                at = around(sums, 32, 15)
                local = dotg(
                    (query * jnp.exp(at)).astype(BF16), (key * jnp.exp(-at)).astype(BF16), DT
                )
                total = jnp.where(near, local, 0.0)
                for size, at, mask in ((64, 31, middle), (128, 63, far)):
                    f = jnp.exp(-jnp.abs(around(sums, size, at)))
                    wide = dotg((query * f).astype(BF16), (key * f).astype(BF16), DT)
                    total = jnp.where(mask, wide, total)
                p[c] = total.astype(BF16)
            return carry

        lax.fori_loop(start, stop, step, 0, unroll=4)

    def gated(self, first, count):
        r = self.r

        def step(i, carry):
            c = first + i
            rows = rows_of(c)
            before_state = r["m3r"][...].astype(F32).reshape(CH, 256)
            for width, b, s, e, p, t, h in self.heads:
                state = s[c] + jnp.exp(e[pl.ds(c, 1), :]) * before_state[:, h * KA : h * KA + width]
                out = dot(p[c], r["v"][h, rows, :]) + dotg(t[rows, :], state.astype(BF16), DT)
                inverse = lax.rsqrt(jnp.mean(out * out, axis=-1, keepdims=True) + EPS)
                gate = r["og"][h, rows, :].astype(F32)
                normed = out * inverse * r["gain"][h : h + 1, :]
                value = gate * jax.nn.sigmoid(gate) * normed
                r["gat"][rows, h * CH : (h + 1) * CH] = value.astype(BF16)
            return carry

        lax.fori_loop(0, count, step, 0, unroll=2)


HALF = 1024
BLK = 256
LEFT, RIGHT = slice(0, 512), slice(512, 1024)


class Reduce:
    def __init__(self, net, part, comb, hop, joined, direct):
        self.net, self.part, self.comb = net, part, comb
        self.hop, self.joined, self.direct = hop, joined, direct
        n = net.number
        self.h = [[n(), n()] for _ in range(2)]
        self.j = [[n(), n()] for _ in range(2)]
        self.d = [[n(), n()] for _ in range(2)]

    def send_far(self, *pieces):
        net = self.net
        for piece in pieces:
            rows = pl.ds(piece * CH, CH)
            for side, (k, cols) in enumerate(((1, LEFT), (-1, RIGHT))):
                net.send(
                    self.part.at[0, rows, cols],
                    self.hop.at[side, rows],
                    self.h[side][piece],
                    net.to_x(k),
                )

    def send_near(self, *pieces):
        net = self.net
        for piece in pieces:
            rows = pl.ds(piece * CH, CH)
            for side, (k, block, cols) in enumerate(((1, 1, RIGHT), (-1, 2, LEFT))):
                net.send(
                    self.part.at[block, rows, cols],
                    self.direct.at[side, rows],
                    self.d[side][piece],
                    net.to_x(k),
                )

    def join(self, *pieces):
        net = self.net
        for piece in pieces:
            rows = slice(piece * CH, (piece + 1) * CH)
            for side, (k, block, cols) in enumerate(((1, 1, LEFT), (-1, 2, RIGHT))):
                net.arrived(self.hop.at[side, rows], self.h[side][piece])
                both = self.part[block, rows, cols].astype(F32) + self.hop[side, rows, :].astype(
                    F32
                )
                self.comb[side, rows, :] = both.astype(BF16)
                net.send(
                    self.comb.at[side, rows],
                    self.joined.at[side, rows],
                    self.j[side][piece],
                    net.to_x(k),
                )

    def arrived(self, piece):
        net = self.net
        rows = slice(piece * CH, (piece + 1) * CH)
        for side in range(2):
            net.arrived(self.direct.at[side, rows], self.d[side][piece])
            net.arrived(self.joined.at[side, rows], self.j[side][piece])

    def total(self, own, rows):
        left = (
            own[rows, LEFT]
            + self.joined[0, rows, :].astype(F32)
            + self.direct[1, rows, :].astype(F32)
        )
        right = (
            own[rows, RIGHT]
            + self.joined[1, rows, :].astype(F32)
            + self.direct[0, rows, :].astype(F32)
        )
        return left, right


class Feed:
    def __init__(self, net, r):
        self.net, self.r = net, r
        n = net.number
        self.n_res, self.n_wo, self.n_out = n(), n(), n()
        self.n_ss = [n(), n()]
        self.n_dp = [n() for _ in range(4)]
        self.n_gat = [n() for _ in range(NX)]
        self.n_hid = [[n(), n()] for _ in range(NX)]
        self.ring = [[n(), n()] for _ in range(2)]
        self.far = [[n(), n()] for _ in range(2)]
        self.over = [[n(), n()] for _ in range(NX)]
        self.first = Reduce(net, r["p1"], r["c1"], r["h1"], r["j1"], r["d1"])
        self.second = Reduce(net, r["p2"], r["c2"], r["h2"], r["j2"], r["d2"])

    def cols(self, core):
        return pl.ds(pl.multiple_of(core * HALF, HALF), HALF)

    def block(self, k):
        return rows_of(self.net.at_x(k), BLK)

    def swap_inputs(self):
        net, r = self.net, self.r
        other = 1 - net.c
        net.send(
            r["res"].at[:, self.cols(other)], r["base"].at[net.c], self.n_res, net.partner()
        )
        net.send(r["wo"].at[:, :, self.cols(other)], r["wop"], self.n_wo, net.partner())

    def send_gated(self, k):
        net, r = self.net, self.r
        rows = self.block(k)
        net.send(r["gat"].at[rows], r["gatp"].at[rows], self.n_gat[k % NX], net.partner())

    def swapped_inputs(self):
        net, r = self.net, self.r
        net.arrived(r["wop"], self.n_wo)
        net.arrived(r["base"].at[1 - net.c], self.n_res)
        r["base"][net.c] = r["res"][:, self.cols(net.c)]

    def project(self, k):
        net, r = self.net, self.r
        rows = self.block(k)
        net.arrived(r["gatp"].at[rows], self.n_gat[k % NX])
        mine, theirs = r["gat"][rows, :], r["gatp"][rows, :]
        for side in range(2):
            cols = slice(side * 512, (side + 1) * 512)
            at = pl.ds(pl.multiple_of(net.c * HALF + side * 512, 512), 512)
            part = dot(mine, r["wo"][:, :, at].reshape(2 * CH, 512)) + dot(
                theirs, r["wop"][:, :, cols].reshape(2 * CH, 512)
            )
            if k == 0:
                r["own1"][:, cols] = part
            else:
                r["p1"][{2: 0, 1: 1, -1: 2}[k], :, cols] = part.astype(BF16)

    def middle(self, piece):
        net, r = self.net, self.r
        self.first.arrived(piece)
        rows = slice(piece * CH, (piece + 1) * CH)
        left, right = self.first.total(r["own1"], rows)
        base = r["base"].at[piece]
        mid_l = (base[:, LEFT].astype(F32) + left).astype(BF16)
        mid_r = (base[:, RIGHT].astype(F32) + right).astype(BF16)
        r["mid"][rows, LEFT] = mid_l
        r["mid"][rows, RIGHT] = mid_r
        mid_l, mid_r = mid_l.astype(F32), mid_r.astype(F32)
        squares = jnp.sum(mid_l * mid_l + mid_r * mid_r, axis=-1, keepdims=True)
        r["ss"][piece] = jnp.broadcast_to(squares, (CH, 128))
        net.send(r["ss"].at[piece], r["ssp"].at[piece], self.n_ss[piece], net.partner())
        net.arrived(r["ssp"].at[piece], self.n_ss[piece])
        inverse = lax.rsqrt((squares + r["ssp"][piece][:, 0:1]) * (1.0 / 2048.0) + EPS)
        gain = r["fgain"][:, self.cols(net.c)]
        start = pl.multiple_of(net.x * BLK + piece * CH, CH)
        for side, mid in ((LEFT, mid_l), (RIGHT, mid_r)):
            normed = (mid * inverse * gain[:, side]).astype(BF16)
            r["all"][net.c, pl.ds(start, CH), side] = normed

    def piece(self, k, half, side=slice(0, HALF), other=False):
        start = pl.multiple_of(self.net.at_x(k) * BLK + half * CH, CH)
        core = 1 - self.net.c if other else self.net.c
        return self.r["all"].at[core, pl.ds(start, CH), side]

    def over_send(self, k, half):
        part = self.piece(k, half)
        self.net.send(part, part, self.over[k % NX][half], self.net.partner())

    def over_wait(self, *pieces):
        for k, half in pieces:
            self.net.arrived(self.piece(k, half, other=True), self.over[k % NX][half])

    def rows_out(self, half):
        net = self.net
        part = self.piece(0, half)
        for d, k in enumerate((1, -1)):
            net.send(part, part, self.ring[d][half], net.to_x(k))
        self.over_send(0, half)

    def rows_on(self, half):
        net = self.net
        for d, (k, side) in enumerate(((1, LEFT), (-1, RIGHT))):
            net.arrived(self.piece(-k, half), self.ring[d][half])
            part = self.piece(-k, half, side)
            net.send(part, part, self.far[d][half], net.to_x(k))
            self.over_send(-k, half)

    def rows_far(self, half):
        for d, side in enumerate((LEFT, RIGHT)):
            self.net.arrived(self.piece(2, half, side), self.far[d][half])
        self.over_send(2, half)

    def rows(self, k, half):
        start = pl.multiple_of(self.net.at_x(k) * BLK + half * CH, CH)
        return pl.ds(start, CH)

    def hidden(self, *pieces):
        net, r = self.net, self.r
        self.over_wait(*pieces)
        blocks = [self.rows(*piece) for piece in pieces]

        def step(n, carry):
            at = pl.ds(pl.multiple_of(n * 256, 256), 256)
            lines = jnp.concatenate(
                [
                    jnp.concatenate([r["all"][0, rows, :], r["all"][1, rows, :]], axis=1)
                    for rows in blocks
                ],
                axis=0,
            )
            gate, up = (
                dot(lines, r["wg"][:, :, low : low + 64, at].reshape(2 * HALF, 256))
                for low in (0, UP)
            )
            value = (gate * jax.nn.sigmoid(gate) * up).astype(BF16)
            for i, rows in enumerate(blocks):
                r["hid"][rows, at] = value[i * CH : (i + 1) * CH]
            return carry

        lax.fori_loop(0, FF // 256, step, 0)
        for (k, half), rows in zip(pieces, blocks):
            net.send(
                r["hid"].at[rows], r["hidp"].at[rows], self.n_hid[k % NX][half], net.partner()
            )

    def swap_tile(self, kz):
        net, r = self.net, self.r
        z = net.at_z(kz)

        @pl.when(z // 4 == 1 - net.c)
        def _():
            n = lax.rem(z, 4)
            self.tile(z, n).start()

    def tile(self, z, n):
        r = self.r
        return self.net._copy(
            r["wg"].at[z, :, DOWN:], r["dp"].at[n], self.n_dp[0] + n, self.net.partner()
        )

    def swapped_down(self):
        for n in range(4):
            copy = self.tile(4 * (1 - self.net.c) + n, n)
            copy.wait_send()
            copy.wait_recv()

    def down(self, *pieces):
        net, r = self.net, self.r
        blocks = [self.rows(*piece) for piece in pieces]
        for (k, half), rows in zip(pieces, blocks):
            net.arrived(r["hidp"].at[rows], self.n_hid[k % NX][half])

        def step(n, carry):
            at = pl.ds(pl.multiple_of(n * 256, 256), 256)
            lines = jnp.concatenate(
                [
                    jnp.concatenate([r["hid"][rows, :], r["hidp"][rows, :]], axis=1)
                    for rows in blocks
                ],
                axis=0,
            )
            w = jnp.concatenate(
                [
                    r["wg"][4 * net.c + n, :, DOWN:, :].reshape(256, FF),
                    r["dp"][n].reshape(256, FF),
                ],
                axis=1,
            )
            part = dotg(lines, w, DT)
            for i, (k, half) in enumerate(pieces):
                mine = part[i * CH : (i + 1) * CH]
                rows = slice(half * CH, (half + 1) * CH)
                if k == 0:
                    r["own2"][rows, at] = mine
                else:
                    r["p2"][{2: 0, 1: 1, -1: 2}[k], rows, at] = mine.astype(BF16)
            return carry

        lax.fori_loop(0, HALF // 256, step, 0)

    def finish(self):
        net, r = self.net, self.r
        for piece in range(2):
            self.second.arrived(piece)
            rows = slice(piece * CH, (piece + 1) * CH)
            left, right = self.second.total(r["own2"], rows)
            r["outs"][piece, :, LEFT] = (r["mid"][rows, LEFT].astype(F32) + left).astype(BF16)
            r["outs"][piece, :, RIGHT] = (r["mid"][rows, RIGHT].astype(F32) + right).astype(BF16)
        net.send(r["outs"].at[1 - net.c], r["outp"], self.n_out, net.partner())

        @pl.when(net.c == 0)
        def _():
            r["lo"][...] = r["outs"][0]

        @pl.when(net.c == 1)
        def _():
            r["hi"][...] = r["outs"][1]

        net.arrived(r["outp"], self.n_out)

        @pl.when(net.c == 0)
        def _():
            r["hi"][...] = r["outp"][...]

        @pl.when(net.c == 1)
        def _():
            r["lo"][...] = r["outp"][...]


INPUTS = dict(
    ga=((1024, KA), BF16),
    gb=((KB, 1024), BF16),
    fade=((NCH, CH), F32),
    ka=((1024, KA), BF16),
    kb=((KB, 1024), BF16),
    v=((2, 1024, CH), BF16),
    gate=None,
    down=None,
    up=None,
    qa=((1024, KA), BF16),
    qb=((KB, 1024), BF16),
    res=((CH, 2048), BF16),
    wo=((2, CH, 2048), BF16),
    og=((2, 1024, CH), BF16),
    gain=((2, CH), F32),
    fgain=((1, 2048), F32),
)
SCRATCH = dict(
    wg=((NZ, NY, WR, FF), BF16),
    ba=((1024, KA), F32),
    bb=((1024, KB), F32),
    sa=((NCH, CH, KA), F32),
    sb=((NCH, CH, KB), F32),
    ea=((NCH, KA), F32),
    eb=((NCH, KB), F32),
    pa=((NCH, CH, CH), BF16),
    pb=((NCH, CH, CH), BF16),
    ta=((1024, KA), BF16),
    tb=((1024, KB), BF16),
    m1s=((NY, 48, 256), BF16),
    m1r=((NY, 48, 256), BF16),
    m2s=((48, 256), BF16),
    m2r=((NZ, 48, 256), BF16),
    m3s=((NY, 32, 256), BF16),
    m3r=((NY, 32, 256), BF16),
    gat=((1024, 256), BF16),
    gatp=((1024, 256), BF16),
    wop=((2, CH, HALF), BF16),
    base=((2, CH, HALF), BF16),
    own1=((BLK, HALF), F32),
    p1=((3, BLK, HALF), BF16),
    c1=((2, BLK, 512), BF16),
    h1=((2, BLK, 512), BF16),
    j1=((2, BLK, 512), BF16),
    d1=((2, BLK, 512), BF16),
    mid=((BLK, HALF), BF16),
    ss=((2, CH, 128), F32),
    ssp=((2, CH, 128), F32),
    all=((2, 1024, HALF), BF16),
    hid=((1024, FF), BF16),
    hidp=((1024, FF), BF16),
    dp=((4, NY, 64, FF), BF16),
    own2=((BLK, HALF), F32),
    p2=((3, BLK, HALF), BF16),
    c2=((2, BLK, 512), BF16),
    h2=((2, BLK, 512), BF16),
    j2=((2, BLK, 512), BF16),
    d2=((2, BLK, 512), BF16),
    outs=((2, CH, HALF), BF16),
    outp=((CH, HALF), BF16),
)
COPIES = 192


class Inputs:
    def __init__(self, net, r, given, sems):
        self.copies = {}
        for i, name in enumerate(INPUTS):
            if INPUTS[name] is None:
                lo = {"gate": 0, "up": UP, "down": DOWN}[name]
                dst = r["wg"].at[net.z, net.y, lo : lo + 64]
            else:
                dst = r[name]
            self.copies[name] = pltpu.make_async_copy(given[name], dst, sems.at[i])

    def fetch(self, *names):
        for name in names:
            self.copies[name].start()

    def ready(self, *names):
        for name in names:
            self.copies[name].wait()


def kernel(*refs):
    count = len(INPUTS)
    given = dict(zip(INPUTS, refs))
    held = [name for name in INPUTS if INPUTS[name] is not None]
    r = dict(zip(["lo", "hi"] + list(SCRATCH) + held, refs[count:]))
    isem, ssem, rsem = refs[-3:]
    net = Net(ssem, rsem)
    weights = Weights(net, r["wg"])
    attention = Attention(net, r)
    feed = Feed(net, r)
    assert net.count <= COPIES, net.count
    inputs = Inputs(net, r, given, isem)
    inputs.fetch("ga", "gb", "fade", "ka", "kb", "v")
    net.greet()
    inputs.ready("ga", "gb", "fade", "ka", "kb", "v")
    inputs.fetch("gate", "up", "down", "qa", "qb", "res", "wo", "og", "gain", "fgain")
    attention.states()
    inputs.ready("gate", "up", "down", "qa", "qb", "res", "wo", "og", "gain", "fgain")
    net.greeted()
    attention.send_quarters()
    weights.yz_send(1)
    weights.x_out()
    weights.yb_send(UP, 0)
    feed.swap_inputs()
    attention.scores(0, 8)
    attention.send_line_total()
    weights.x_forward()
    weights.yb_send(DOWN, 0)
    weights.yz_wait(1)
    weights.yz_send(2)
    weights.yb_send(UP, 1, -1)
    weights.x_forwarded()
    weights.xz_send(1)
    feed.swapped_inputs()
    attention.send_incoming()
    attention.incoming()
    for k in (2, 1, -1, 0):
        attention.gated(2 * net.at_x(k), 2)
        feed.send_gated(k)
        if k == 1:
            feed.project(2)
            feed.first.send_far(0, 1)
    feed.project(1)
    feed.project(-1)
    feed.first.send_near(0, 1)
    feed.project(0)
    weights.yz_wait(2)
    weights.yz_send(3)
    weights.yb_send(UP, 2, -2)
    weights.yf_send(UP, 0, 1, -1)
    weights.yb_send(DOWN, 1, -1)
    weights.xz_wait(1)
    weights.xz_send(2)
    weights.yz_wait(3)
    weights.yz_send(4)
    weights.yb_send(UP, 3, -3)
    weights.yb_send(DOWN, 2, -2)
    feed.first.join(0, 1)
    weights.yf_send(UP, 2, -2)
    weights.xz_wait(2)
    weights.xz_send(3)
    weights.yz_wait(4)
    weights.yb_send(UP, 4)
    weights.yb_send(DOWN, 3, -3, 4)
    feed.middle(0)
    feed.rows_out(0)
    feed.middle(1)
    feed.rows_out(1)
    feed.rows_on(0)
    weights.yf_send(UP, 3, -3)
    weights.xz_wait(3)
    weights.xz_send(4)
    feed.rows_on(1)
    weights.yf_send(UP, 4)
    weights.yf_send(DOWN, 0, 1, -1, 2, -2, 3, -3)
    weights.xz_wait(4)
    weights.yf_wait(UP, 0, 1, -1, 2, -2, 3, -3, 4)
    feed.hidden((1, 0), (-1, 0))
    weights.yf_send(DOWN, 4)
    feed.hidden((1, 1), (-1, 1))
    feed.rows_far(0)
    for k in (0, 1, -1, 2, -2, 3, -3, 4):
        weights.yf_wait(DOWN, k)
        feed.swap_tile(k)
    feed.swapped_down()
    feed.down((1, 0), (-1, 0))
    feed.second.send_near(0)
    feed.down((1, 1), (-1, 1))
    feed.second.send_near(1)
    feed.rows_far(1)
    feed.hidden((2, 0), (2, 1))
    feed.hidden((0, 0), (0, 1))
    feed.down((2, 0), (2, 1))
    feed.second.send_far(0, 1)
    feed.down((0, 0), (0, 1))
    feed.second.join(0, 1)
    feed.finish()
    net.drain()


def per_device(
    residual,
    first_group_queries,
    first_group_keys,
    second_group_queries,
    second_group_keys,
    primary_retain_switch_inputs,
    secondary_retain_switch_inputs,
    timestep_fading_exponent,
    values,
    output_gate_logits,
    head_norm_gains,
    output_projection,
    feedforward_norm_gain,
    gate_projection,
    up_projection,
    down_projection,
):
    given = dict(
        ga=primary_retain_switch_inputs,
        gb=secondary_retain_switch_inputs.T,
        fade=timestep_fading_exponent.reshape(NCH, CH),
        ka=first_group_keys,
        kb=second_group_keys.T,
        v=values,
        gate=gate_projection,
        down=down_projection.T,
        up=up_projection,
        qa=first_group_queries,
        qb=second_group_queries.T,
        res=residual,
        wo=output_projection,
        og=output_gate_logits,
        gain=head_norm_gains,
        fgain=feedforward_norm_gain.reshape(1, -1),
    )
    half = jax.ShapeDtypeStruct((CH, HALF), BF16)
    buffers = list(SCRATCH.values()) + [spec for spec in INPUTS.values() if spec is not None]
    lo, hi = pl.pallas_call(
        kernel,
        out_shape=(half, half),
        in_specs=[pl.BlockSpec(memory_space=pl.ANY)] * len(INPUTS),
        out_specs=(pl.BlockSpec(memory_space=pltpu.VMEM),) * 2,
        scratch_shapes=[pltpu.VMEM(shape, dtype) for shape, dtype in buffers]
        + [
            pltpu.SemaphoreType.DMA((len(INPUTS),)),
            pltpu.SemaphoreType.DMA((COPIES,)),
            pltpu.SemaphoreType.DMA((COPIES,)),
        ],
        compiler_params=pltpu.CompilerParams(
            collective_id=0, has_side_effects=True, vmem_limit_bytes=66000000
        ),
    )(*(given[name] for name in INPUTS))
    return jnp.concatenate([lo, hi], axis=1)


def solution(mesh):
    finer = Mesh(mesh.devices.reshape(NZ, NY, NX, 2), SP_TP)
    return jax.shard_map(
        per_device,
        mesh=finer,
        in_specs=(
            P(SP_TP, None),
            P(SP, TP),
            P(SP, TP),
            P(SP, TP),
            P(SP, TP),
            P(SP, TP),
            P(SP, TP),
            P(SP),
            P(None, SP, TP),
            P(None, SP, TP),
            P(None, TP),
            P(None, TP, None),
            P(),
            P(SP, TP),
            P(SP, TP),
            P(TP, SP),
        ),
        out_specs=P(SP_TP, None),
        check_vma=False,
    )
```

time: 119 us -> 111 us (0.933)
  local copies, waits for them, and re-layouts: 5.54 us -> 0 us
  Pallas kernels: 112 us -> 109 us
    unnamed x14 -> x0, local copies, waits for them, and re-layouts: 5.54 us -> none
    pallas_call x1, Pallas kernels: 112 us -> 109 us  [per_device(): pl.pallas_call(kernel, out_shape=(half, half), in_specs=[pl.BlockSpec(mem...]
where the time goes in v2:
time: 111 us
  Pallas kernels  109 us (98%)
  other arithmetic  1.86 us (2%)
    pallas_call x1, Pallas kernels, per_device(): pl.pallas_call(kernel, out_shape=(half, half), in_specs=[pl.BlockSpec(mem...  109 us

profile of v2, /device:TPU:1, one launch (start us, length us, event | category | flops | bytes accessed | tf_op | source)
XLA Modules:
  0.0 111.2 jit_solution(4159298250837628305)
XLA Ops:
  0.0 109.3 %shard_map.154 = (bf16[128,1024]{1,0:T(8,128)(2,1)}, bf16[128,1024]{1,0:T(8,128)(2,1)}) custom-call(bf16[1024,128]{1,0:T(8,128)(2,1)} %refs_0_.1, bf16[64,1024]{1,0:T(8,128)(2,1)} %bitcast.6, f32[8,128]{1,0:T(8,128)} %bitcast.11, bf16[1024,128]{1,0:T(8,128)(2,1)} %refs_3_.1, bf16[64,1024]{1,0:T(8,128)(2,1)} %bitcast.7, bf16[2,1024,128]{2,1,0:T(8,128)(2,1)} %refs_5_.1, ...), custom_call_target="tpu_custom_call" | custom-call | tf_op jit(solution)/shard_map/pallas_call | solution.py:900
  109.3 1.9 %pad_maximum_fusion = bf16[128,2048]{1,0:T(8,128)(2,1)} fusion(bf16[128,1024]{1,0:T(8,128)(2,1)} %get-tuple-element.8, bf16[128,1024]{1,0:T(8,128)(2,1)} %get-tuple-element.7), kind=kLoop, calls=%fused_computation | loop fusion | flops 1048576 | bytes 1048576 | tf_op jit(solution)/shard_map/concatenate | solution.py:915

commit v3 on v2

--- a/solution.py
+++ b/solution.py
@@ -261,7 +261,7 @@
 
     def send_quarters(self):
         net, r = self.net, self.r
-        for k in range(1, NY):
+        for k in (2, 1, 3):
             net.send(r["m1s"].at[net.at_y(k)], r["m1r"].at[k], self.m1[k], net.to_y(k))
 
     @staticmethod
@@ -289,15 +289,25 @@
         high = decay.astype(BF16).astype(F32)
         r["m2s"][0:quarter, :] = state.astype(BF16)
         r["m2s"][quarter:, :] = jnp.where(row16 == 0, high, decay - high).astype(BF16)
-        for k in (1, -1, 2, -2, 3, -3, 4):
-            net.send(r["m2s"], r["m2r"].at[k % NZ], self.m2[k % NZ], net.to_z(k))
+        for k in (4, 3, 5, 2, 6, 1, 7):
+
+            @pl.when(net.z + k < NZ)
+            def _():
+                self.line_copy(k).start()
+
+    def line_copy(self, k):
+        net, r = self.net, self.r
+        return net._copy(r["m2s"], r["m2r"].at[k], self.m2[k], net.to_z(k))
 
     def send_incoming(self):
         net, r = self.net, self.r
         quarter = CH // NY
         for k in range(1, NZ):
-            net.arrived(r["m2r"].at[k], self.m2[k])
-        r["m2r"][0] = jnp.zeros((48, 256), BF16)
+
+            @pl.when(k <= net.z)
+            def _():
+                net.arrived(r["m2r"].at[k], self.m2[k])
+
         state = jnp.zeros((quarter, 256), F32)
         for i in range(NZ - 1):
             slot = lax.rem(net.z - i + NZ, NZ)
@@ -308,12 +318,18 @@
             slot = lax.rem(net.y - i + NY, NY)
             own, factor = self.opened(r["m1r"][slot])
             state = factor * state + own
-        for k in range(1, NY):
+        for k in (2, 1, 3):
             net.send(r["m3s"].at[net.at_y(k)], r["m3r"].at[net.y], self.m3[k], net.to_y(k))
         r["m3r"][net.y] = r["m3s"][net.y]
 
     def incoming(self):
         net, r = self.net, self.r
+        for k in range(1, NZ):
+
+            @pl.when(net.z + k < NZ)
+            def _():
+                self.line_copy(k).wait_send()
+
         for k in range(1, NY):
             net.arrived(r["m3r"].at[net.at_y(-k)], self.m3[k])
 
@@ -771,16 +787,17 @@
     feed = Feed(net, r)
     assert net.count <= COPIES, net.count
     inputs = Inputs(net, r, given, isem)
-    inputs.fetch("ga", "gb", "fade", "ka", "kb", "v")
     net.greet()
+    inputs.fetch("gate", "up", "down", "ga", "gb", "fade", "ka", "kb", "v")
     inputs.ready("ga", "gb", "fade", "ka", "kb", "v")
-    inputs.fetch("gate", "up", "down", "qa", "qb", "res", "wo", "og", "gain", "fgain")
-    attention.states()
-    inputs.ready("gate", "up", "down", "qa", "qb", "res", "wo", "og", "gain", "fgain")
+    inputs.fetch("qa", "qb", "res", "wo", "og", "gain", "fgain")
+    inputs.ready("gate", "up", "down")
     net.greeted()
-    attention.send_quarters()
     weights.yz_send(1)
     weights.x_out()
+    attention.states()
+    inputs.ready("qa", "qb", "res", "wo", "og", "gain", "fgain")
+    attention.send_quarters()
     weights.yb_send(UP, 0)
     feed.swap_inputs()
     attention.scores(0, 8)
@@ -793,7 +810,12 @@
     weights.x_forwarded()
     weights.xz_send(1)
     feed.swapped_inputs()
+    weights.yf_send(UP, 0)
     attention.send_incoming()
+    weights.yz_wait(2)
+    weights.yz_send(3)
+    weights.yb_send(DOWN, 1, -1)
+    weights.yb_send(UP, 2, -2)
     attention.incoming()
     for k in (2, 1, -1, 0):
         attention.gated(2 * net.at_x(k), 2)
@@ -805,52 +827,57 @@
     feed.project(-1)
     feed.first.send_near(0, 1)
     feed.project(0)
-    weights.yz_wait(2)
-    weights.yz_send(3)
-    weights.yb_send(UP, 2, -2)
-    weights.yf_send(UP, 0, 1, -1)
-    weights.yb_send(DOWN, 1, -1)
+    weights.yf_send(UP, 1, -1)
     weights.xz_wait(1)
     weights.xz_send(2)
+    weights.yf_send(DOWN, 0)
     weights.yz_wait(3)
     weights.yz_send(4)
     weights.yb_send(UP, 3, -3)
     weights.yb_send(DOWN, 2, -2)
+    weights.yf_send(UP, 2, -2)
     feed.first.join(0, 1)
-    weights.yf_send(UP, 2, -2)
+    weights.yb_send(DOWN, 3, -3)
+    weights.yf_send(DOWN, 1, -1)
     weights.xz_wait(2)
     weights.xz_send(3)
+    feed.middle(0)
+    feed.rows_out(0)
     weights.yz_wait(4)
     weights.yb_send(UP, 4)
-    weights.yb_send(DOWN, 3, -3, 4)
-    feed.middle(0)
-    feed.rows_out(0)
+    weights.yb_send(DOWN, 4)
     feed.middle(1)
     feed.rows_out(1)
+    weights.yf_send(UP, 3, -3)
+    weights.yf_send(DOWN, 2, -2)
     feed.rows_on(0)
-    weights.yf_send(UP, 3, -3)
     weights.xz_wait(3)
     weights.xz_send(4)
+    weights.yf_send(UP, 4)
+    weights.yf_send(DOWN, 3, -3, 4)
     feed.rows_on(1)
-    weights.yf_send(UP, 4)
-    weights.yf_send(DOWN, 0, 1, -1, 2, -2, 3, -3)
+    for k in (0, 1, -1):
+        weights.yf_wait(DOWN, k)
+        feed.swap_tile(k)
+    weights.yf_wait(UP, 0, 1, -1, 2, -2, 3, -3, 4)
     weights.xz_wait(4)
-    weights.yf_wait(UP, 0, 1, -1, 2, -2, 3, -3, 4)
     feed.hidden((1, 0), (-1, 0))
-    weights.yf_send(DOWN, 4)
+    for k in (2, -2):
+        weights.yf_wait(DOWN, k)
+        feed.swap_tile(k)
     feed.hidden((1, 1), (-1, 1))
     feed.rows_far(0)
-    for k in (0, 1, -1, 2, -2, 3, -3, 4):
+    feed.hidden((0, 0), (0, 1))
+    for k in (3, -3, 4):
         weights.yf_wait(DOWN, k)
         feed.swap_tile(k)
+    feed.rows_far(1)
+    feed.hidden((2, 0), (2, 1))
     feed.swapped_down()
     feed.down((1, 0), (-1, 0))
     feed.second.send_near(0)
     feed.down((1, 1), (-1, 1))
     feed.second.send_near(1)
-    feed.rows_far(1)
-    feed.hidden((2, 0), (2, 1))
-    feed.hidden((0, 0), (0, 1))
     feed.down((2, 0), (2, 1))
     feed.second.send_far(0, 1)
     feed.down((0, 0), (0, 1))

time: 111 us -> 106 us (0.955)
  Pallas kernels: 109 us -> 104 us
    pallas_call x1, Pallas kernels: 109 us -> 104 us  [per_device(): pl.pallas_call(kernel, out_shape=(half, half), in_specs=[pl.BlockSpec(mem...]
where the time goes in v3:
time: 106 us
  Pallas kernels  104 us (98%)
  other arithmetic  1.86 us (2%)
    pallas_call x1, Pallas kernels, per_device(): pl.pallas_call(kernel, out_shape=(half, half), in_specs=[pl.BlockSpec(mem...  104 us

profile of v3, /device:TPU:1, one launch (start us, length us, event | category | flops | bytes accessed | tf_op | source)
XLA Modules:
  0.0 106.1 jit_solution(8048755670068794773)
XLA Ops:
  0.0 104.2 %shard_map.154 = (bf16[128,1024]{1,0:T(8,128)(2,1)}, bf16[128,1024]{1,0:T(8,128)(2,1)}) custom-call(bf16[1024,128]{1,0:T(8,128)(2,1)} %refs_0_.1, bf16[64,1024]{1,0:T(8,128)(2,1)} %bitcast.6, f32[8,128]{1,0:T(8,128)} %bitcast.11, bf16[1024,128]{1,0:T(8,128)(2,1)} %refs_3_.1, bf16[64,1024]{1,0:T(8,128)(2,1)} %bitcast.7, bf16[2,1024,128]{2,1,0:T(8,128)(2,1)} %refs_5_.1, ...), custom_call_target="tpu_custom_call" | custom-call | tf_op jit(solution)/shard_map/pallas_call | solution.py:927
  104.2 1.9 %pad_maximum_fusion = bf16[128,2048]{1,0:T(8,128)(2,1)} fusion(bf16[128,1024]{1,0:T(8,128)(2,1)} %get-tuple-element.8, bf16[128,1024]{1,0:T(8,128)(2,1)} %get-tuple-element.7), kind=kLoop, calls=%fused_computation | loop fusion | flops 1048576 | bytes 1048576 | tf_op jit(solution)/shard_map/concatenate | solution.py:942
